TPU v7x, 256 devices: a whole 4x4x8 slice. The times are simulated.
256 devices in a mesh: ep: 64 (over z, x, core), tp: 4 (over y).
Axes of the slice: x: 4, y: 4, z: 8, core: 2. Of those that a mesh axis runs over, the one named last changes fastest.
Arguments:
- projected_queries: bfloat16 [16384, 2048], P('ep', 'tp'), may hold values from -245 to 245, as said below
- key_proj: bfloat16 [16384, 512], P('ep', 'tp'), may hold values from -6.2 to 6.2
- projected_values: bfloat16 [16384, 512], P('ep', 'tp'), may hold values from -24 to 24
- head_sink_logits: float32 [32], P('tp'), may hold values from 1 to 6
- out_weight: bfloat16 [2048, 4096], P('tp'), may hold values from -0.125 to 0.125
- expert_input: bfloat16 [8192, 4096], P('ep'), may hold values from -6 to 6
- norm_gain: float32 [4096], replicated, may hold values from 0.1 to 1.9
- routing: int32 [8192, 4], P('ep'), may hold values from 0 to 63, all different within a row; in each aligned block of 128 rows (0 to 127, 128 to 255, ...) at most 12 rows name the same one
- route_weight: float32 [8192, 4], P('ep'), may hold values from 0.1 to 1
- gate_weight: bfloat16 [64, 4096, 1024], P('ep', None, 'tp'), may hold values from -0.27929688 to 0.27929688
- up_weight: bfloat16 [64, 4096, 1024], P('ep', None, 'tp'), may hold values from -0.27929688 to 0.27929688
- down_weight: bfloat16 [64, 1024, 4096], P('ep', 'tp'), may hold values from -0.046875 to 0.046875
Outputs:
- mixer_output: bfloat16 [16384, 4096], P(('ep', 'tp'))
- expert_output: bfloat16 [8192, 4096], P('ep', 'tp')
Inputs may be any that keep to these rules, and one draw needn't show every extreme that they name: `projected_queries`: in the hidden draw some queries nearly equal a large multiple of a nearby key. `routing`: each row names 4 different experts; among the rows of one device (aligned blocks of 128 rows) no expert is named more than 12 times, a bound that some block reaches.
All inputs are finite; a program needn't handle non-finite values.
Results may differ from a plain program's by a relative error of at most 0.014.
Values may be sent and summed in bfloat16 or wider, within the bound.
A program may use at most 128 MiB of HBM per device.

v0:
```python
import jax
import jax.numpy as jnp
from jax import lax
from jax.sharding import PartitionSpec as P

D = 4096
HEAD_SIZE = 64
WINDOW_KEYS = 128
TOPK = 4


EPS = 1e-06
CLAMP = 7.0
SLOPE = 1.702


def passed_along(block, axis, distance):
    devices = range(lax.axis_size(axis))
    route = [(i - distance, i) for i in devices if i - distance in devices]
    return lax.ppermute(block, axis, route)


def shards(
    projected_queries,
    key_proj,
    projected_values,
    head_sink_logits,
    out_weight,
    expert_input,
    norm_gain,
    routing,
    route_weight,
    gate_weight,
    up_weight,
    down_weight,
):
    query_rows = projected_queries.shape[0]
    kv_heads = key_proj.shape[1] // HEAD_SIZE
    heads_per_group = projected_queries.shape[1] // HEAD_SIZE // kv_heads
    count_of_blocks = query_rows // WINDOW_KEYS
    prior_key, prior_value = passed_along(
        (key_proj[query_rows - WINDOW_KEYS :], projected_values[query_rows - WINDOW_KEYS :]),
        "ep",
        1,
    )
    key_all = jnp.concatenate([prior_key, key_proj], axis=0)
    value_all = jnp.concatenate([prior_value, projected_values], axis=0)
    window_keys = jnp.concatenate(
        [
            key_all[:-WINDOW_KEYS].reshape(count_of_blocks, WINDOW_KEYS, kv_heads, HEAD_SIZE),
            key_all[WINDOW_KEYS:].reshape(count_of_blocks, WINDOW_KEYS, kv_heads, HEAD_SIZE),
        ],
        axis=1,
    )
    window_values = jnp.concatenate(
        [
            value_all[:-WINDOW_KEYS].reshape(count_of_blocks, WINDOW_KEYS, kv_heads, HEAD_SIZE),
            value_all[WINDOW_KEYS:].reshape(count_of_blocks, WINDOW_KEYS, kv_heads, HEAD_SIZE),
        ],
        axis=1,
    )
    query_blocks = projected_queries.reshape(
        count_of_blocks, WINDOW_KEYS, kv_heads, heads_per_group, HEAD_SIZE
    )
    scores = jnp.einsum(
        "nqhgd,nshd->nhgqs", query_blocks, window_keys, preferred_element_type=jnp.float32
    ) * HEAD_SIZE ** (-0.5)
    offset = lax.axis_index("ep") * query_rows
    block_ids = jnp.arange(count_of_blocks)[:, None, None] * WINDOW_KEYS + offset
    query_pos = block_ids + jnp.arange(WINDOW_KEYS)[None, :, None]
    key_pos = block_ids - WINDOW_KEYS + jnp.arange(2 * WINDOW_KEYS)[None, None, :]
    permitted_mask = (key_pos <= query_pos) & (query_pos - key_pos < WINDOW_KEYS) & (key_pos >= 0)
    scores = jnp.where(permitted_mask[:, None, None, :, :], scores, -jnp.inf)
    sink_col = head_sink_logits.reshape(kv_heads, heads_per_group)[None, :, :, None, None]
    highest = jnp.maximum(jnp.max(scores, axis=-1, keepdims=True), sink_col)
    numerator = jnp.exp(scores - highest)
    denominator = jnp.sum(numerator, axis=-1, keepdims=True) + jnp.exp(sink_col - highest)
    weights = (numerator / denominator).astype(jnp.bfloat16)
    attended = jnp.einsum(
        "nhgqs,nshd->nqhgd", weights, window_values, preferred_element_type=jnp.float32
    )
    attended = attended.astype(jnp.bfloat16).reshape(
        query_rows, kv_heads * heads_per_group * HEAD_SIZE
    )
    mixer_output = lax.psum_scatter(
        jnp.dot(attended, out_weight, preferred_element_type=jnp.float32).astype(jnp.bfloat16),
        "tp",
        scatter_dimension=0,
        tiled=True,
    )
    token_rows = expert_input.shape[0]
    experts = lax.axis_size("ep")
    capacity = max(3 * token_rows * TOPK // (2 * experts), 2)
    col_share = D // lax.axis_size("tp")
    widened = expert_input.astype(jnp.float32)
    normed = (
        widened
        * lax.rsqrt(jnp.mean(widened * widened, axis=-1, keepdims=True) + EPS)
        * norm_gain[None, :]
    ).astype(jnp.bfloat16)
    flat_ids = routing.reshape(-1)
    onehot = (flat_ids[:, None] == jnp.arange(experts, dtype=jnp.int32)[None, :]).astype(jnp.int32)
    rank_in = jnp.cumsum(onehot, axis=0) - 1
    target = flat_ids * capacity + jnp.sum(rank_in * onehot, axis=1)
    tok_ids = jnp.arange(token_rows * TOPK) // TOPK
    slot_tok = jnp.full((experts * capacity,), token_rows, jnp.int32).at[target].set(tok_ids)
    gate_one = gate_weight[0]
    up_one = up_weight[0]
    own_cols = lax.dynamic_slice_in_dim(normed, lax.axis_index("tp") * col_share, col_share, 1)
    extended = jnp.concatenate([own_cols, jnp.zeros((1, col_share), jnp.bfloat16)], axis=0)
    outgoing = jnp.take(extended, slot_tok, axis=0).reshape(experts, capacity, col_share)
    arrived = lax.all_to_all(outgoing, "ep", split_axis=0, concat_axis=0, tiled=True).reshape(
        experts * capacity, col_share
    )
    portion = lax.all_gather(arrived, "tp", axis=1, tiled=True)
    gate_pre = jnp.dot(portion, gate_one, preferred_element_type=jnp.float32)
    up_pre = jnp.dot(portion, up_one, preferred_element_type=jnp.float32)
    gate_cut = jnp.minimum(gate_pre, CLAMP)
    activated = (
        (jnp.clip(up_pre, -CLAMP, CLAMP) + 1.0) * gate_cut * jax.nn.sigmoid(SLOPE * gate_cut)
    ).astype(jnp.bfloat16)
    down_cols = lax.all_to_all(down_weight[0], "tp", split_axis=1, concat_axis=0, tiled=True)
    expert_result = jnp.dot(
        lax.all_gather(activated, "tp", axis=1, tiled=True),
        down_cols,
        preferred_element_type=jnp.float32,
    ).astype(jnp.bfloat16)
    returned = lax.all_to_all(
        expert_result.reshape(experts, capacity, col_share),
        "ep",
        split_axis=0,
        concat_axis=0,
        tiled=True,
    )
    picked = jnp.take(returned.reshape(experts * capacity, col_share), target, axis=0)
    picked = picked.astype(jnp.float32).reshape(token_rows, TOPK, col_share)
    expert_output = jnp.sum(picked * route_weight[:, :, None], axis=1).astype(jnp.bfloat16)
    return (mixer_output, expert_output)


def solution(mesh):
    placed = (
        P("ep", "tp"),
        P("ep", "tp"),
        P("ep", "tp"),
        P("tp"),
        P("tp", None),
        P("ep", None),
        P(),
        P("ep", None),
        P("ep", None),
        P("ep", None, "tp"),
        P("ep", None, "tp"),
        P("ep", "tp", None),
    )
    return jax.shard_map(
        shards,
        mesh=mesh,
        in_specs=placed,
        out_specs=(P(("ep", "tp"), None), P("ep", "tp")),
        check_vma=False,
    )
```

profile of v0, /device:TPU:2, one launch (start us, length us, event | category | flops | bytes accessed | tf_op | source)
XLA Modules:
  0.0 303.8 jit_solution(12836123487075077681)
XLA Ops:
  7.2 2.9 convert_element_type.41
  10.2 0.3 multiply_reduce_fusion.1
  10.5 0.1 copy.66
  10.6 0.1 eq.26
  10.7 0.1 reshape.223
  10.9 1.2 reduce-window.6
  12.1 0.2 slice_reduce_fusion
  12.3 0.1 copy.71
  12.4 0.1 mul.95
  12.6 0.1 fusion.32
  12.7 2.4 scatter_custom_fusion
  15.2 0.7 dynamic-slice
  15.9 1.1 fusion.25
  17.1 3.6 %gather_fusion = bf16[768,1024]{1,0:T(8,128)(2,1)} fusion(bf16[129,1024]{1,0:T(8,128)(2,1)S(1)} %concatenate.19, s32[1024]{0:T(1024)S(1)} %pad_clamp_fusion.1), kind=kCustom, calls=%fused_computation | custom fusion | bytes 3148800 | tf_op jit(solution)/shard_map/jit(_take)/gather | solution.py:111
  20.6 3.6 %gather.13 = bf16[64,12,1024]{2,1,0:T(8,128)(2,1)} reshape(bf16[768,1024]{1,0:T(8,128)(2,1)} %gather_fusion) | data formatting | bytes 3145728 | tf_op jit(solution)/shard_map/jit(_take)/gather | solution.py:111
  24.2 0.1 broadcast_in_dim.55
  24.4 1.9 broadcast_select_fusion
  26.2 63.2 %all_to_all.29 = bf16[64,12,1024]{2,1,0:T(8,128)(2,1)} all-to-all(bf16[64,12,1024]{2,1,0:T(8,128)(2,1)S(1)} %broadcast_select_fusion), channel_id=1, replica_groups=mesh['ep'=64,'tp'=4] {'ep'}, dimensions={0} | all-to-all | bytes 3145728 | tf_op jit(solution)/shard_map/all_to_all | solution.py:112
  89.4 3.6 %reshape.225 = bf16[768,1024]{1,0:T(8,128)(2,1)} reshape(bf16[64,12,1024]{2,1,0:T(8,128)(2,1)} %all_to_all.29) | data formatting | bytes 3145728 | tf_op jit(solution)/shard_map/reshape | solution.py:112
  93.0 4.1 %copy.72 = bf16[1,256,4096]{1,2,0:T(8,128)(2,1)} copy(bf16[1,256,4096]{2,1,0:T(8,128)(2,1)} %param.23) | data formatting | bytes 4194304 | tf_op args[11]
  97.1 4.6 %all-to-all-start.1 = ((bf16[256,4,1024]{0,2,1:T(8,128)(2,1)}), bf16[256,4,1024]{0,2,1:T(8,128)(2,1)}, u32[]{:S(2)}, u32[]{:S(2)}) async-start(bf16[256,4,1024]{0,2,1:T(8,128)(2,1)} %bitcast.66), calls=%async_computation.2 | async-start | bytes 4194304 | tf_op jit(solution)/shard_map/all_to_all | solution.py:122
  101.8 1.9 collective-permute-start.1
  103.7 3.5 %collective-permute-start = (bf16[128,128]{1,0:T(8,128)(2,1)S(1)}, bf16[128,128]{1,0:T(8,128)(2,1)S(1)}, u32[]{:S(2)}, u32[]{:S(2)}) collective-permute-start(bf16[128,128]{1,0:T(8,128)(2,1)S(1)} %slice.18), channel_id=1, source_target_pairs={{0,4},{4,8},{8,12},{12,16},{16,20},{20,24},{24,28},{28,32},{32,36}... | collective-permute-start | bytes 98312 | tf_op jit(solution)/shard_map/ppermute | solution.py:20
  107.2 0.1 broadcast_compare_fusion
  107.3 0.1 iota_add_fusion
  107.4 70.1 %all-gather.3.cloned.1.call-done = bf16[768,4096]{1,0:T(8,128)(2,1)} async-done(((bf16[768,1024]{1,0:T(8,128)(2,1)}), bf16[768,4096]{1,0:T(8,128)(2,1)}) %all-gather.3.cloned.1.call-update) | async-done | bytes 6291472 | tf_op jit(solution)/shard_map/all_gather | solution.py:115
  177.5 4.7 %fusion.8 = f32[768,256]{1,0:T(8,128)S(1)} fusion(bf16[768,4096]{1,0:T(8,128)(2,1)} %all-gather.3.cloned.1.call-done, bf16[1,4096,256]{2,1,0:T(8,128)(2,1)S(1)} %copy-done), kind=kOutput, calls=%fused_computation.17 | convolution fusion | flops 1610809344 | bytes 9175040 | tf_op jit(solution)/shard_map/dot_general | solution.py:116
  182.2 0.5 copy-done.10
  182.7 2.6 fusion.20
  185.3 0.2 reduce-scatter.2.cloned.1.call-start
  185.6 0.1 iota_add_fusion.1
  185.7 0.2 fusion.30
  185.9 0.1 reshape.258
  186.0 0.1 reshape.256
  186.1 0.3 reshape.259
  186.4 0.1 copy.61
  186.5 0.1 max.24
  186.6 0.1 copy.57
  186.7 0.1 reshape.257
  186.8 0.1 copy.60
  186.9 1.9 fusion.45
  188.8 0.1 broadcast_maximum_fusion
  188.9 0.1 reshape.255
  189.0 0.1 copy.56
  189.1 2.0 fusion.4
  191.1 0.1 exponential_add_fusion
  191.2 0.1 copy-done.3
  191.3 0.5 fusion.23
  191.8 0.3 copy.65
  192.1 1.5 copy-done.2
  193.6 2.7 convolution_convert_fusion
  196.3 4.0 %copy.73 = bf16[4,256,1024]{2,1,0:T(8,128)(2,1)} copy(bf16[4,256,1024]{1,2,0:T(8,128)(2,1)} %bitcast.12) | data formatting | bytes 4194304 | tf_op jit(solution)/shard_map/all_to_all | solution.py:122
  200.3 13.5 %all-gather.5.cloned.1.call-done = bf16[768,1024]{1,0:T(8,128)(2,1)} async-done(((bf16[768,256]{1,0:T(8,128)(2,1)}), bf16[768,1024]{1,0:T(8,128)(2,1)}) %all-gather.5.cloned.1.call-update) | async-done | bytes 1572880 | tf_op jit(solution)/shard_map/all_gather | solution.py:124
  213.8 5.0 %convolution_convert_fusion.1 = bf16[768,1024]{1,0:T(8,128)(2,1)} fusion(bf16[768,1024]{1,0:T(8,128)(2,1)} %all-gather.5.cloned.1.call-done, bf16[1024,1024]{1,0:T(8,128)(2,1)} %bitcast.67), kind=kOutput, calls=%fused_computation.15 | convolution fusion | flops 1611399168 | bytes 5242880 | tf_op jit(solution)/shard_map/dot_general | solution.py:123
  218.8 3.6 %reshape.226 = bf16[64,12,1024]{2,1,0:T(8,128)(2,1)} reshape(bf16[768,1024]{1,0:T(8,128)(2,1)} %convolution_convert_fusion.1) | data formatting | bytes 3145728 | tf_op jit(solution)/shard_map/reshape | solution.py:129
  222.4 10.9 %all-to-all-start.2 = ((bf16[64,12,1024]{2,1,0:T(8,128)(2,1)}), bf16[64,12,1024]{2,1,0:T(8,128)(2,1)}, u32[]{:S(2)}, u32[]{:S(2)}) async-start(bf16[64,12,1024]{2,1,0:T(8,128)(2,1)} %reshape.226), calls=%async_computation.3 | async-start | bytes 4194304 | tf_op jit(solution)/shard_map/all_to_all | solution.py:128
  233.2 0.1 reduce_sum.42
  233.4 0.1 copy.70
  233.6 0.1 copy.74
  233.7 50.7 %all-to-all-done.2 = bf16[64,12,1024]{2,1,0:T(8,128)(2,1)} async-done(((bf16[64,12,1024]{2,1,0:T(8,128)(2,1)}), bf16[64,12,1024]{2,1,0:T(8,128)(2,1)}, u32[]{:S(2)}, u32[]{:S(2)}) %all-to-all-start.2) | async-done | bytes 1572896 | tf_op jit(solution)/shard_map/all_to_all | solution.py:128
  284.4 3.6 %reshape.227 = bf16[768,1024]{1,0:T(8,128)(2,1)} reshape(bf16[64,12,1024]{2,1,0:T(8,128)(2,1)} %all-to-all-done.2) | data formatting | bytes 3145728 | tf_op jit(solution)/shard_map/reshape | solution.py:135
  288.0 4.3 %gather_fusion.1 = bf16[512,1024]{1,0:T(8,128)(2,1)S(1)} fusion(bf16[768,1024]{1,0:T(8,128)(2,1)} %reshape.227, s32[1024]{0:T(1024)S(1)} %pad_clamp_fusion), kind=kCustom, calls=%fused_computation.1 | custom fusion | bytes 2099200 | tf_op jit(solution)/shard_map/jit(_take)/gather | solution.py:135
  292.4 1.2 gather.15
  293.6 3.6 %multiply_reduce_fusion = bf16[128,1024]{1,0:T(8,128)(2,1)} fusion(f32[128,4]{1,0:T(8,128)S(1)} %copy.74, bf16[128,4,1024]{2,1,0:T(4,128)(2,1)} %gather.15, pred[128,4]{1,0:T(8,128)(4,1)S(1)} %copy.70), kind=kLoop, calls=%fused_computation.9 | loop fusion | flops 1966080 | bytes 1313280 | tf_op jit(solution)/shard_map/reduce_sum | solution.py:137
  (49 shorter events, 0.4 us)
Async XLA Ops:
  7.2 170.3 %copy-start = (bf16[1,4096,256]{2,1,0:T(8,128)(2,1)S(1)}, bf16[1,4096,256]{2,1,0:T(8,128)(2,1)}, u32[]{:S(2)}) copy-start(bf16[1,4096,256]{2,1,0:T(8,128)(2,1)} %param.21) | copy-start | bytes 6291460
  7.2 3.0 copy-start.1
  7.2 170.3 %all-gather.3.cloned.1.call-start = ((), (), s32[]{:S(2)}) async-start(), calls=%async_computation.5 | async-start | bytes 7864320 | tf_op jit(solution)/shard_map/all_gather | solution.py:115
  7.2 3.2 %copy-start.7 = (s32[128,4]{0,1:T(4,128)S(1)}, s32[128,4]{0,1:T(4,128)}, u32[]{:S(2)}) copy-start(s32[128,4]{0,1:T(4,128)} %param.19) | copy-start | bytes 6148
  97.1 4.6 %copy-start.4 = (bf16[256,128]{1,0:T(8,128)(2,1)S(1)}, bf16[256,128]{1,0:T(8,128)(2,1)}, u32[]{:S(2)}) copy-start(bf16[256,128]{1,0:T(8,128)(2,1)} %param.13) | copy-start | bytes 196612
  97.1 6.6 %copy-start.5 = (bf16[256,128]{1,0:T(8,128)(2,1)S(1)}, bf16[256,128]{1,0:T(8,128)(2,1)}, u32[]{:S(2)}) copy-start(bf16[256,128]{1,0:T(8,128)(2,1)} %param.14) | copy-start | bytes 196612
  97.1 99.2 %all-to-all-start.1 = ((bf16[256,4,1024]{0,2,1:T(8,128)(2,1)}), bf16[256,4,1024]{0,2,1:T(8,128)(2,1)}, u32[]{:S(2)}, u32[]{:S(2)}) async-start(bf16[256,4,1024]{0,2,1:T(8,128)(2,1)} %bitcast.66), calls=%async_computation.2 | async-start | bytes 4194304 | tf_op jit(solution)/shard_map/all_to_all | solution.py:122
  101.7 112.1 %all-gather.5.cloned.1.call-start = ((), (), s32[]{:S(2)}) async-start(), calls=%async_computation.6 | async-start | bytes 1966080 | tf_op jit(solution)/shard_map/all_gather | solution.py:124
  101.8 84.9 %collective-permute-start.1 = (bf16[128,128]{1,0:T(8,128)(2,1)S(1)}, bf16[128,128]{1,0:T(8,128)(2,1)S(1)}, u32[]{:S(2)}, u32[]{:S(2)}) collective-permute-start(bf16[128,128]{1,0:T(8,128)(2,1)S(1)} %slice.20), channel_id=1, source_target_pairs={{0,4},{4,8},{8,12},{12,16},{16,20},{20,24},{24,28},{28,32},{32,36}... | collective-permute-start | bytes 98312 | tf_op jit(solution)/shard_map/ppermute | solution.py:20
  103.7 85.1 %collective-permute-start = (bf16[128,128]{1,0:T(8,128)(2,1)S(1)}, bf16[128,128]{1,0:T(8,128)(2,1)S(1)}, u32[]{:S(2)}, u32[]{:S(2)}) collective-permute-start(bf16[128,128]{1,0:T(8,128)(2,1)S(1)} %slice.18), channel_id=1, source_target_pairs={{0,4},{4,8},{8,12},{12,16},{16,20},{20,24},{24,28},{28,32},{32,36}... | collective-permute-start | bytes 98312 | tf_op jit(solution)/shard_map/ppermute | solution.py:20
  177.5 4.7 %copy-start.9 = (bf16[768,4096]{1,0:T(8,128)(2,1)S(1)}, bf16[768,4096]{1,0:T(8,128)(2,1)}, u32[]{:S(2)}) copy-start(bf16[768,4096]{1,0:T(8,128)(2,1)} %all-gather.3.cloned.1.call-done) | copy-start | bytes 18874372
  177.5 5.2 %copy-start.10 = (bf16[1,4096,256]{2,1,0:T(8,128)(2,1)S(1)}, bf16[1,4096,256]{2,1,0:T(8,128)(2,1)}, u32[]{:S(2)}) copy-start(bf16[1,4096,256]{2,1,0:T(8,128)(2,1)} %param.22) | copy-start | bytes 6291460
  182.7 3.4 %copy-start.6 = (bf16[256,512]{1,0:T(8,128)(2,1)S(1)}, bf16[256,512]{1,0:T(8,128)(2,1)}, u32[]{:S(2)}) copy-start(bf16[256,512]{1,0:T(8,128)(2,1)} %param.12) | copy-start | bytes 786436
  182.7 3.8 %copy-start.11 = (f32[8]{0:T(128)S(1)}, f32[8]{0:T(128)}, u32[]{:S(2)}) copy-start(f32[8]{0:T(128)} %param.15) | copy-start | bytes 100
  185.3 111.9 %reduce-scatter.2.cloned.1.call-start = ((), (), s32[]{:S(2)}) async-start(), calls=%async_computation.4 | async-start | bytes 2621440 | tf_op jit(solution)/shard_map/reduce_scatter | solution.py:85
  189.1 2.2 copy-start.3
  191.3 2.3 copy-start.2
  222.4 11.2 %copy-start.8 = (f32[128,4]{0,1:T(4,128)S(1)}, f32[128,4]{0,1:T(4,128)}, u32[]{:S(2)}) copy-start(f32[128,4]{0,1:T(4,128)} %param.20) | copy-start | bytes 6148
  222.4 62.0 %all-to-all-start.2 = ((bf16[64,12,1024]{2,1,0:T(8,128)(2,1)}), bf16[64,12,1024]{2,1,0:T(8,128)(2,1)}, u32[]{:S(2)}, u32[]{:S(2)}) async-start(bf16[64,12,1024]{2,1,0:T(8,128)(2,1)} %reshape.226), calls=%async_computation.3 | async-start | bytes 4194304 | tf_op jit(solution)/shard_map/all_to_all | solution.py:128
Sparse Core Ops, SparseCore 0:
  93.2 84.2 all-gather.2
  185.5 28.2 all-gather.4
  216.9 33.2 reduce-scatter.1
where the time goes:
time: 305 us; the launch traced here: 304 us
  waiting for transfers between devices  134 us (44%)
  blocking collectives  63.2 us (21%)
  local copies, waits for them, and re-layouts  39.7 us (13%)
  starting transfers between devices  21.2 us (7%)
  matrix products  17.4 us (6%)
  between operations  14.2 us (5%)
  other arithmetic  13.9 us (5%)
    all_gather x1, waiting for transfers between devices, shards(): portion = lax.all_gather(arrived, 'tp', axis=1, tiled=True)  70.1 us
    all_to_all x1, blocking collectives, shards(): lax.all_to_all(outgoing, 'ep', split_axis=0, concat_axis=0, tiled=True)  63.2 us
    all_to_all x1, waiting for transfers between devices, shards(): lax.all_to_all(expert_result.reshape(experts, capacity, col_share), 'ep',...  50.7 us
    all_gather x1, waiting for transfers between devices, shards(): lax.all_gather(activated, 'tp', axis=1, tiled=True)  13.5 us
    all_to_all x1, starting transfers between devices, shards(): lax.all_to_all(expert_result.reshape(experts, capacity, col_share), 'ep',...  10.9 us
    gather x2, local copies, waits for them, and re-layouts, shards(): jnp.take(extended, slot_tok, axis=0).reshape(experts, capacity, col_share)  7.16 us
    unnamed x27, local copies, waits for them, and re-layouts  6.43 us
  transfers between devices with their start and end apart: 7, of which 3 were waited for; matrix products, arithmetic and copies ran while one was open for 15% of the time, Pallas kernels for 0%

commit v1 on v0

v1 whole, which is shorter than its diff:
```python
import jax
import jax.numpy as jnp
from jax import lax
from jax.experimental import pallas as pl
from jax.experimental.pallas import tpu as pltpu
from jax.sharding import PartitionSpec as P

EPS = 1e-06
CLAMP = 7.0
SLOPE = 1.702

NZ = 8
NQ = 8
NY = 4
D = 4096
TOK = 128
CAP = 12
ROWS = NZ * CAP
FC = 256
C = 8
HID = 256
NB = 4
MESH = pl.DeviceIdType.MESH
F32 = jnp.float32
BF16 = jnp.bfloat16


def kernel(
    q_ref, k_ref, v_ref, sink_ref, wo_hbm, x_ref, gain_ref, rt_ref, rw_ref, wg_hbm, wu_hbm, wd_hbm,
    mix_ref, out_ref,
    G, XS, XF, XO, WG, WU, WO, DN, S, CM, INFOS, IR, ACCG, ACCU, ACT, YS, RX, SR, RR,
    KP, KX, VX, ATT, PT, PM,
    ls, zss, zrs, iss, irs, xss, xrs, yss, yrs, dss, drs, ass, ars, wss, wrs, sss, srs, mss, mrs, hss, hrs,
):
    ep = lax.axis_index("ep")
    y = lax.axis_index("tp")
    z = ep // NQ
    q = lax.rem(ep, NQ)
    half = lax.rem(y, 2)

    def wrap(a, n):
        return lax.rem(a + n, n)

    def at_z(zz):
        return (zz * NQ + q, y)

    def at_q(qq):
        return (z * NQ + qq, y)

    def at_y(yy):
        return (ep, yy)

    def remote(src, dst, ss, rs, dev):
        return pltpu.make_async_remote_copy(src, dst, ss, rs, device_id=dev, device_id_type=MESH)

    barrier = pltpu.get_barrier_semaphore()
    next_ep, prev_ep = wrap(ep + 1, NZ * NQ), wrap(ep - 1, NZ * NQ)
    for i in range(1, NZ):
        pl.semaphore_signal(barrier, inc=1, device_id=at_z(wrap(z + i, NZ)), device_id_type=MESH)
    for i in range(1, NQ):
        pl.semaphore_signal(barrier, inc=1, device_id=at_q(wrap(q + i, NQ)), device_id_type=MESH)
    for i in range(1, NY):
        pl.semaphore_signal(barrier, inc=1, device_id=at_y(wrap(y + i, NY)), device_id_type=MESH)
    for e in (next_ep, prev_ep):
        pl.semaphore_signal(barrier, inc=1, device_id=(e, y), device_id_type=MESH)

    loads = [
        pltpu.make_async_copy(wg_hbm, WG, ls.at[0]),
        pltpu.make_async_copy(wu_hbm, WU, ls.at[1]),
        pltpu.make_async_copy(wo_hbm, WO, ls.at[2]),
        pltpu.make_async_copy(wd_hbm.at[:, pl.ds(pl.multiple_of(y * 1024, 1024), 1024)], DN.at[y], ls.at[3]),
    ]
    for load in loads:
        load.start()

    def mean_step(j, total):
        w = x_ref[:, pl.ds(pl.multiple_of(j * 512, 512), 512)].astype(F32)
        return total + jnp.sum(w * w, axis=1, keepdims=True)

    total = lax.fori_loop(0, D // 512, mean_step, jnp.zeros((TOK, 1), F32))
    scale = lax.rsqrt(total * (1.0 / D) + EPS)

    def norm_step(j, _):
        cols = pl.ds(pl.multiple_of(half * (C * FC) + j * FC, FC), FC)
        G[j, z] = (x_ref[:, cols].astype(F32) * scale * gain_ref[:, cols]).astype(BF16)
        return 0

    lax.fori_loop(0, C, norm_step, 0)

    lane = lax.broadcasted_iota(jnp.int32, (TOK, 128), 1)
    sub = lax.broadcasted_iota(jnp.int32, (TOK, 128), 0)
    expert = lane & 63
    named = jnp.zeros((TOK, 128), F32)
    weight = jnp.zeros((TOK, 128), F32)
    for k in range(4):
        hit = (rt_ref[:, k : k + 1] == expert).astype(F32)
        named = named + hit
        weight = weight + hit * rw_ref[:, k : k + 1]
    earlier = (lane < sub).astype(F32).astype(BF16)
    rank = jnp.dot(earlier, named.astype(BF16), preferred_element_type=F32)
    info = jnp.where(lane < 64, jnp.where(named > 0.5, rank, -1.0), weight).T
    INFOS[:, 0:8, :] = info[:64].reshape(NZ, 8, 128)
    INFOS[:, 8:16, :] = info[64:].reshape(NZ, 8, 128)
    IR[z] = INFOS[z]

    def z_copy(j, s, d):
        if d == 0:
            origin, peer = wrap(z - s, NZ), wrap(z + 1, NZ)
        else:
            origin, peer = wrap(z + s, NZ), wrap(z - 1, NZ)
        return remote(G.at[j, origin], G.at[j, origin], zss.at[d, s, j], zrs.at[d, s, j], at_z(peer))

    def i_copy(i):
        to = wrap(z + i, NZ)
        return remote(INFOS.at[to], IR.at[z], iss.at[i], irs.at[i], at_z(to))

    def x_copy(j, to):
        i = wrap(to - q, NQ)
        return remote(XS.at[j, to], XF.at[j, q], xss.at[j, i], xrs.at[j, i], at_q(to))

    def y_copy(j, d):
        to = wrap(y + 1, NY) if d == 0 else wrap(y - 1, NY)
        part = pl.ds(4 * d, 4)
        return remote(XF.at[j, part], XO.at[j, part], yss.at[d, j], yrs.at[d, j], at_y(to))

    def d_copy(i):
        to = wrap(y + i, NY)
        src = wd_hbm.at[:, pl.ds(pl.multiple_of(to * 1024, 1024), 1024)]
        return remote(src, DN.at[y], dss.at[i], drs.at[i], at_y(to))

    def a_copy(r, i):
        to = wrap(y + i, NY)
        part = pl.ds(2 * r, 2)
        return remote(ACT.at[y, part], ACT.at[y, part], ass.at[i, r], ars.at[i, r], at_y(to))

    def w_copy(n, to):
        i = wrap(to - q, NQ)
        return remote(YS.at[n, to], RX.at[n, q], wss.at[n, i], wrs.at[n, i], at_q(to))

    def s_copy(n, s, d):
        peer = wrap(z + 1, NZ) if d == 0 else wrap(z - 1, NZ)
        return remote(SR.at[d, n, s], RR.at[d, n, s], sss.at[d, n, s], srs.at[d, n, s], at_z(peer))

    def m_copy(i):
        to = wrap(y + i, NY)
        return remote(PT.at[to], PM.at[i], mss.at[i], mrs.at[i], at_y(to))

    halo = [
        remote(k_ref.at[pl.ds(128, 128)], KP.at[0], hss.at[0], hrs.at[0], (next_ep, y)),
        remote(v_ref.at[pl.ds(128, 128)], KP.at[1], hss.at[1], hrs.at[1], (next_ep, y)),
    ]

    pl.semaphore_wait(barrier, (NZ - 1) + (NQ - 1) + (NY - 1) + 2)
    for d in range(2):
        z_copy(0, 0, d).start()
    for i in range(1, NZ):
        i_copy(i).start()
    for copy in halo:
        copy.start()
    for i in (2, 1, 3):
        d_copy(i).start()
    ACCG[...] = jnp.zeros_like(ACCG)
    ACCU[...] = jnp.zeros_like(ACCU)

    def build_windows():
        for copy in halo:
            copy.wait_recv()
        lanes = lax.broadcasted_iota(jnp.int32, (384, 128), 1)
        for t, (ref, wide) in enumerate(((k_ref, KX), (v_ref, VX))):
            whole = jnp.concatenate([KP[t], ref[...]], axis=0).astype(F32)
            turned = pltpu.roll(whole, 64, 1)
            zero = jnp.zeros_like(whole)
            wide[0, 0] = jnp.where(lanes < 64, whole, zero).astype(BF16)
            wide[1, 1] = jnp.where(lanes < 64, zero, whole).astype(BF16)
            wide[0, 1] = jnp.where(lanes < 64, zero, turned).astype(BF16)
            wide[1, 0] = jnp.where(lanes < 64, turned, zero).astype(BF16)

    def div12(a):
        return (a * 5462) >> 16

    def build_gather():
        for i in range(1, NZ):
            i_copy(i).wait_recv()
        row = lax.broadcasted_iota(jnp.int32, (ROWS, 128), 0)
        row_z = div12(row)
        row_k = (row - row_z * CAP).astype(F32)

        def step(zs, _):
            cols = pl.ds(pl.multiple_of(zs * TOK, TOK), TOK)
            ranks = IR[zs, 0:8, :]
            for e in range(NQ):
                hit = (row_z == zs) & (ranks[e : e + 1, :] == row_k)
                S[e, :, cols] = hit.astype(F32).astype(BF16)
            return 0

        lax.fori_loop(0, NZ, step, 0)

    def build_combine():
        i16 = lax.broadcasted_iota(jnp.int32, (16, NQ * ROWS), 0)
        col = lax.broadcasted_iota(jnp.int32, (16, NQ * ROWS), 1)
        col_q = (div12(col)) >> 3
        spread_rank = (i16 == col_q).astype(F32).astype(BF16)
        spread_weight = (i16 == col_q + 8).astype(F32).astype(BF16)
        col = lax.broadcasted_iota(jnp.int32, (TOK, NQ * ROWS), 1)
        col12 = div12(col)
        col_z = col12 & 7
        col_k = (col - col12 * CAP).astype(F32)

        def step(zs, _):
            turned = IR[zs].T.astype(BF16)
            ranks = jnp.dot(turned, spread_rank, preferred_element_type=F32)
            weights = jnp.dot(turned, spread_weight, preferred_element_type=F32)
            hit = (col_z == zs) & (ranks == col_k)
            CM[zs] = jnp.where(hit, weights, 0.0).astype(BF16)
            return 0

        lax.fori_loop(0, NZ, step, 0)

    def attend(u):
        n, p = u // 4, lax.rem(u, 4)
        kv = p // 2
        rows = pl.ds(pl.multiple_of(n * 128, 128), 128)
        window = pl.ds(pl.multiple_of(n * 128, 128), 256)
        cols = pl.ds(pl.multiple_of(p * 128, 128), 128)
        queries = q_ref[rows, cols]
        i = lax.broadcasted_iota(jnp.int32, (128, 256), 0)
        s = lax.broadcasted_iota(jnp.int32, (128, 256), 1)
        first = jnp.where((ep == 0) & (n == 0), 128, 0)
        seen = (s > i) & (s <= i + 128) & (s >= first)
        both = jnp.zeros((128, 128), F32)
        for h in range(2):
            scores = lax.dot_general(
                queries, KX[kv, h, window, :], (((1,), (1,)), ((), ())), preferred_element_type=F32
            ) * 0.125
            scores = jnp.where(seen, scores, -jnp.inf)
            sink = sink_ref[2 * p + h]
            highest = jnp.maximum(jnp.max(scores, axis=1, keepdims=True), sink)
            e = jnp.exp(scores - highest)
            under = jnp.sum(e, axis=1, keepdims=True) + jnp.exp(sink - highest)
            w = (e / under).astype(BF16)
            both = both + jnp.dot(w, VX[kv, h, window, :], preferred_element_type=F32)
        ATT[rows, cols] = both.astype(BF16)

    def project(u):
        cols = pl.ds(pl.multiple_of(u * 512, 512), 512)
        part = jnp.dot(ATT[...], WO[:, cols], preferred_element_type=F32).astype(BF16)
        PT[:, :, cols] = part.reshape(NY, 64, 512)

    def expert_dots(src, j, w):
        def step(r, _):
            part = pl.ds(4 * r, 4)
            block = src[j, part].reshape(4 * ROWS, FC)
            rows = pl.ds(pl.multiple_of(r * 4 * ROWS, 4 * ROWS), 4 * ROWS)
            ACCG[rows, :] += jnp.dot(block, WG[w], preferred_element_type=F32)
            ACCU[rows, :] += jnp.dot(block, WU[w], preferred_element_type=F32)
            return 0

        lax.fori_loop(0, 2, step, 0)

    def within(j):
        return (j >= 0) & (j < C)

    def tick(t, _):
        @pl.when(t + 1 < C)
        def _():
            for d in range(2):
                z_copy(t + 1, 0, d).start()

        @pl.when(within(t - 3))
        def _():
            j = t - 3
            for d in range(2):
                z_copy(j, 2, d).wait_recv()

                @pl.when(lax.rem(j, 2) == d)
                def _():
                    z_copy(j, 3, d).start()

        for s in (2, 1):

            @pl.when(within(t - s))
            def _():
                for d in range(2):
                    z_copy(t - s, s - 1, d).wait_recv()
                    z_copy(t - s, s, d).start()

        @pl.when(within(t - 4))
        def _():
            j = t - 4
            for d in range(2):

                @pl.when(lax.rem(j, 2) == d)
                def _():
                    z_copy(j, 3, d).wait_recv()

            def step(r, _):
                part = pl.ds(4 * r, 4)
                block = jnp.dot(
                    S[part].reshape(4 * ROWS, NZ * TOK), G[j].reshape(NZ * TOK, FC), preferred_element_type=F32
                ).astype(BF16)
                XS[j, part] = block.reshape(4, ROWS, FC)
                for i in range(4):

                    @pl.when(4 * r + i != q)
                    def _():
                        x_copy(j, 4 * r + i).start()

                return 0

            lax.fori_loop(0, 2, step, 0)
            XF[j, q] = XS[j, q]

        @pl.when(within(t - 6))
        def _():
            j = t - 6
            for i in range(1, NQ):
                x_copy(j, wrap(q + i, NQ)).wait_recv()
            for d in range(2):
                y_copy(j, d).start()
            @pl.when(j == 0)
            def _():
                loads[0].wait()
                loads[1].wait()
            expert_dots(XF, j, half * C + j)

        @pl.when(within(t - 8))
        def _():
            j = t - 8
            for d in range(2):
                y_copy(j, d).wait_recv()
            expert_dots(XO, j, (1 - half) * C + j)

        @pl.when(t == 0)
        def _():
            build_windows()

        @pl.when(t == 1)
        def _():
            build_gather()

        @pl.when((t >= 2) & (t < 6))
        def _():
            for i in range(2):
                attend((t - 2) * 2 + i)

        @pl.when(t == 6)
        def _():
            loads[2].wait()

        @pl.when((t >= 6) & (t < 10))
        def _():
            for i in range(2):
                project((t - 6) * 2 + i)

        @pl.when(t == 10)
        def _():
            build_combine()

        return 0

    lax.fori_loop(0, C + 8, tick, 0)

    def activate(r, _):
        rows = pl.ds(pl.multiple_of(r * 2 * ROWS, 2 * ROWS), 2 * ROWS)
        g = jnp.minimum(ACCG[rows, :], CLAMP)
        u = jnp.clip(ACCU[rows, :], -CLAMP, CLAMP) + 1.0
        a = (u * g * jax.nn.sigmoid(SLOPE * g)).astype(BF16)
        ACT[y, pl.ds(2 * r, 2)] = a.reshape(2, ROWS, HID)
        for i in (2, 1, 3):
            a_copy(r, i).start()
        return 0

    lax.fori_loop(0, 4, activate, 0)
    for i in (2, 1, 3):
        m_copy(i).start()
    loads[3].wait()
    for i in range(1, NY):
        d_copy(i).wait_recv()

    def arrive(r, _):
        for i in range(1, NY):
            a_copy(r, i).wait_recv()
        return 0

    lax.fori_loop(0, 4, arrive, 0)

    def down(n, _):
        cols = pl.ds(pl.multiple_of(n * FC, FC), FC)

        def step(r, _):
            part = pl.ds(4 * r, 4)
            block = jnp.dot(ACT[0, part].reshape(4 * ROWS, HID), DN[0, :, cols], preferred_element_type=F32)
            for i in range(1, NY):
                block = block + jnp.dot(
                    ACT[i, part].reshape(4 * ROWS, HID), DN[i, :, cols], preferred_element_type=F32
                )
            YS[n, part] = block.astype(BF16).reshape(4, ROWS, FC)
            for i in range(4):

                @pl.when(4 * r + i != q)
                def _():
                    w_copy(n, 4 * r + i).start()

            return 0

        lax.fori_loop(0, 2, step, 0)
        RX[n, q] = YS[n, q]
        return 0

    lax.fori_loop(0, NB, down, 0)

    def partial_sum(n, zd):
        return jnp.dot(CM[zd], RX[n].reshape(NQ * ROWS, FC), preferred_element_type=F32)

    def send_sum(n, s, d):
        odd = lax.rem(n, 2)
        ahead = (4 - odd if d == 0 else 3 + odd) - s
        zd = wrap(z + ahead, NZ) if d == 0 else wrap(z - ahead, NZ)
        value = partial_sum(n, zd)
        if s > 0:
            s_copy(n, s - 1, d).wait_recv()
            value = value + RR[d, n, s - 1].astype(F32)
        SR[d, n, s] = value.astype(BF16)
        s_copy(n, s, d).start()

    def wave(w, _):
        for s in (3, 2, 1, 0):
            n = w - s

            @pl.when((n >= 0) & (n < NB))
            def _():
                if s == 0:
                    for i in range(1, NQ):
                        w_copy(n, wrap(q + i, NQ)).wait_recv()
                for d in range(2):
                    if s < 3:
                        send_sum(n, s, d)
                    else:

                        @pl.when(lax.rem(n, 2) == d)
                        def _():
                            send_sum(n, s, d)

        @pl.when((w - 4 >= 0) & (w - 4 < NB))
        def _():
            n = w - 4
            odd = lax.rem(n, 2)
            value = partial_sum(n, z)
            for d in range(2):
                last = 3 - odd if d == 0 else 2 + odd
                s_copy(n, last, d).wait_recv()
                value = value + RR[d, n, last].astype(F32)
            out_ref[:, pl.ds(pl.multiple_of(n * FC, FC), FC)] = value.astype(BF16)

        return 0

    lax.fori_loop(0, NB + 4, wave, 0)

    for i in range(1, NY):
        m_copy(i).wait_recv()

    def mix(u, _):
        cols = pl.ds(pl.multiple_of(u * 512, 512), 512)
        value = PT[y, :, cols].astype(F32)
        for i in range(1, NY):
            value = value + PM[i, :, cols].astype(F32)
        mix_ref[:, cols] = value.astype(BF16)
        return 0

    lax.fori_loop(0, D // 512, mix, 0)

    def sent_chunk(j, _):
        for d in range(2):
            for s in range(3):
                z_copy(j, s, d).wait_send()

            @pl.when(lax.rem(j, 2) == d)
            def _():
                z_copy(j, 3, d).wait_send()

            y_copy(j, d).wait_send()
        for i in range(1, NQ):
            x_copy(j, wrap(q + i, NQ)).wait_send()
        return 0

    lax.fori_loop(0, C, sent_chunk, 0)

    def sent_block(n, _):
        for d in range(2):
            for s in range(3):
                s_copy(n, s, d).wait_send()

            @pl.when(lax.rem(n, 2) == d)
            def _():
                s_copy(n, 3, d).wait_send()

        for i in range(1, NQ):
            w_copy(n, wrap(q + i, NQ)).wait_send()
        for i in range(1, NY):
            a_copy(n, i).wait_send()
        return 0

    lax.fori_loop(0, NB, sent_block, 0)
    for i in range(1, NZ):
        i_copy(i).wait_send()
    for i in range(1, NY):
        d_copy(i).wait_send()
        m_copy(i).wait_send()
    for copy in halo:
        copy.wait_send()


def shards(
    projected_queries,
    key_proj,
    projected_values,
    head_sink_logits,
    out_weight,
    expert_input,
    norm_gain,
    routing,
    route_weight,
    gate_weight,
    up_weight,
    down_weight,
):
    vmem = pl.BlockSpec(memory_space=pltpu.VMEM)
    hbm = pl.BlockSpec(memory_space=pl.ANY)
    smem = pl.BlockSpec(memory_space=pltpu.SMEM)
    dma = pltpu.SemaphoreType.DMA
    return pl.pallas_call(
        kernel,
        out_shape=(
            jax.ShapeDtypeStruct((64, D), BF16),
            jax.ShapeDtypeStruct((TOK, 1024), BF16),
        ),
        in_specs=[vmem, vmem, vmem, smem, hbm, vmem, vmem, vmem, vmem, hbm, hbm, hbm],
        out_specs=(vmem, vmem),
        scratch_shapes=[
            pltpu.VMEM((C, NZ, TOK, FC), BF16),
            pltpu.VMEM((C, NQ, ROWS, FC), BF16),
            pltpu.VMEM((C, NQ, ROWS, FC), BF16),
            pltpu.VMEM((C, NQ, ROWS, FC), BF16),
            pltpu.VMEM((2 * C, FC, HID), BF16),
            pltpu.VMEM((2 * C, FC, HID), BF16),
            pltpu.VMEM((512, D), BF16),
            pltpu.VMEM((NY, HID, 1024), BF16),
            pltpu.VMEM((NQ, ROWS, NZ * TOK), BF16),
            pltpu.VMEM((NZ, TOK, NQ * ROWS), BF16),
            pltpu.VMEM((NZ, 16, 128), F32),
            pltpu.VMEM((NZ, 16, 128), F32),
            pltpu.VMEM((NQ * ROWS, HID), F32),
            pltpu.VMEM((NQ * ROWS, HID), F32),
            pltpu.VMEM((NY, NQ, ROWS, HID), BF16),
            pltpu.VMEM((NB, NQ, ROWS, FC), BF16),
            pltpu.VMEM((NB, NQ, ROWS, FC), BF16),
            pltpu.VMEM((2, NB, 4, TOK, FC), BF16),
            pltpu.VMEM((2, NB, 4, TOK, FC), BF16),
            pltpu.VMEM((2, 128, 128), BF16),
            pltpu.VMEM((2, 2, 384, 128), BF16),
            pltpu.VMEM((2, 2, 384, 128), BF16),
            pltpu.VMEM((256, 512), BF16),
            pltpu.VMEM((NY, 64, D), BF16),
            pltpu.VMEM((NY, 64, D), BF16),
            dma((4,)),
            dma((2, 4, C)), dma((2, 4, C)),
            dma((NZ,)), dma((NZ,)),
            dma((C, NQ)), dma((C, NQ)),
            dma((2, C)), dma((2, C)),
            dma((NY,)), dma((NY,)),
            dma((NY, 4)), dma((NY, 4)),
            dma((NB, NQ)), dma((NB, NQ)),
            dma((2, NB, 4)), dma((2, NB, 4)),
            dma((NY,)), dma((NY,)),
            dma((2,)), dma((2,)),
        ],
        compiler_params=pltpu.CompilerParams(
            collective_id=0, has_side_effects=True, vmem_limit_bytes=62 * 1024 * 1024
        ),
    )(
        projected_queries,
        key_proj,
        projected_values,
        head_sink_logits,
        out_weight,
        expert_input,
        norm_gain.reshape(1, D),
        routing,
        route_weight,
        gate_weight.reshape(2 * C, FC, HID),
        up_weight.reshape(2 * C, FC, HID),
        down_weight.reshape(HID, D),
    )


def solution(mesh):
    placed = (
        P("ep", "tp"),
        P("ep", "tp"),
        P("ep", "tp"),
        P("tp"),
        P("tp", None),
        P("ep", None),
        P(),
        P("ep", None),
        P("ep", None),
        P("ep", None, "tp"),
        P("ep", None, "tp"),
        P("ep", "tp", None),
    )
    return jax.shard_map(
        shards,
        mesh=mesh,
        in_specs=placed,
        out_specs=(P(("ep", "tp"), None), P("ep", "tp")),
        check_vma=False,
    )
```

time: 305 us -> 161 us (0.53)
  Pallas kernels: 0 us -> 152 us
  waiting for transfers between devices: 134 us -> 0 us
  blocking collectives: 63.2 us -> 0 us
  local copies, waits for them, and re-layouts: 39.7 us -> 6.37 us
  starting transfers between devices: 21.2 us -> 0 us
  matrix products: 17.4 us -> 0 us
  other arithmetic: 13.9 us -> 0 us
  between operations: 14.2 us -> 0.64 us
    pallas_call x0 -> x1, Pallas kernels: none -> 152 us  [shards(): pl.pallas_call(kernel, out_shape=(jax.ShapeDtypeStruct((64, D), BF16), ja...]
    all_gather x2 -> x0, waiting for transfers between devices: 83.6 us -> none  [the longest x1 70.1 us: shards(): portion = lax.all_gather(arrived, 'tp', axis=1, tiled=True)]
    all_to_all x1 -> x0, blocking collectives: 63.2 us -> none  [shards(): lax.all_to_all(outgoing, 'ep', split_axis=0, concat_axis=0, tiled=True)]
    all_to_all x2 -> x0, waiting for transfers between devices: 50.7 us -> none  [the longest x1 50.7 us: shards(): lax.all_to_all(expert_result.reshape(experts, capacity, col_share), 'ep',...]
    dot_general x6 -> x0, matrix products: 17.4 us -> none  [the longest x1 5 us: shards(): jnp.dot(lax.all_gather(activated, 'tp', axis=1, tiled=True), down_cols, p...]
    all_to_all x2 -> x0, starting transfers between devices: 15.5 us -> none  [the longest x1 10.9 us: shards(): lax.all_to_all(expert_result.reshape(experts, capacity, col_share), 'ep',...]
    gather x4 -> x0, local copies, waits for them, and re-layouts: 12.7 us -> none  [the longest x2 7.16 us: shards(): jnp.take(extended, slot_tok, axis=0).reshape(experts, capacity, col_share)]
    reshape x13 -> x0, local copies, waits for them, and re-layouts: 12 us -> none  [the longest x1 3.63 us: shards(): returned.reshape(experts * capacity, col_share)]
  transfers between devices with their start and end apart: 7 -> 0, of which waited for: 3 -> 0; matrix products, arithmetic and copies ran while one was open for 15% -> 0% of each run, Pallas kernels for 0% -> 0%
where the time goes in v1:
time: 161 us; the launch traced here: 159 us
  Pallas kernels  152 us (94%)
  local copies, waits for them, and re-layouts  6.37 us (4%)
    pallas_call x1, Pallas kernels, shards(): pl.pallas_call(kernel, out_shape=(jax.ShapeDtypeStruct((64, D), BF16), ja...  152 us
    unnamed x4, local copies, waits for them, and re-layouts  6.37 us

profile of v1, /device:TPU:2, one launch (start us, length us, event | category | flops | bytes accessed | tf_op | source)
XLA Modules:
  0.0 159.2 jit_solution(6970596802881291249)
XLA Ops:
  0.6 1.4 copy.14.rt_ref
  2.0 1.4 copy.15.rw_ref
  3.5 152.2 %shard_map.131 = (bf16[64,4096]{1,0:T(8,128)(2,1)}, bf16[128,1024]{1,0:T(8,128)(2,1)}) custom-call(bf16[256,512]{1,0:T(8,128)(2,1)} %q_ref.1, bf16[256,128]{1,0:T(8,128)(2,1)} %k_ref.1, bf16[256,128]{1,0:T(8,128)(2,1)} %v_ref.1, f32[8]{0:T(128)} %sink_ref.1, bf16[512,4096]{1,0:T(8,128)(2,1)} %wo_hbm.1, bf16[128,4096]{1,0:T(8,128)(2,1)} %x_ref.1, ...), custom_call_target="tpu_custom_call" | custom-call | tf_op jit(solution)/shard_map/pallas_call | solution.py:531
  155.7 1.9 %copy.18 = bf16[64,4096]{1,0:T(8,128)(2,1)} copy(bf16[64,4096]{1,0:T(8,128)(2,1)} %get-tuple-element.4) | data formatting | bytes 1048576
  157.5 1.7 %copy.19 = bf16[128,1024]{1,0:T(8,128)(2,1)} copy(bf16[128,1024]{1,0:T(8,128)(2,1)} %get-tuple-element.5) | data formatting | bytes 524288

commit v2 on v1

v2 whole, which is shorter than its diff:
```python
import jax
import jax.numpy as jnp
from jax import lax
from jax.experimental import pallas as pl
from jax.experimental.pallas import tpu as pltpu
from jax.sharding import PartitionSpec as P

EPS = 1e-06
CLAMP = 7.0
SLOPE = 1.702

NZ = 8
NQ = 8
NY = 4
D = 4096
TOK = 128
CAP = 12
ROWS = NZ * CAP
FC = 256
CE = 7
C = 9
AHEAD = 2
HID = 256
NB = 4
MESH = pl.DeviceIdType.MESH
F32 = jnp.float32
BF16 = jnp.bfloat16


def kernel(
    q_hbm, k_hbm, v_hbm, sink_ref, wo_hbm, x_hbm, gain_hbm, rt_hbm, rw_hbm, wg_hbm, wu_hbm, wd_hbm,
    mix_ref, out_ref,
    q_ref, k_ref, v_ref, x_ref, gain_ref, rt_ref, rw_ref,
    G, XS, XF, XO, W, WO, DN, S, CM, IR, RANK, ACC, ACT, YS, RX, SR, RR,
    KP, KX, VX, ATT, PT, PM,
    ls, zss, zrs, iss, irs, xss, xrs, yss, yrs, dss, drs, ass, ars, wss, wrs, sss, srs, mss, mrs, hss, hrs,
):
    ep = lax.axis_index("ep")
    y = lax.axis_index("tp")
    z = ep // NQ
    q = lax.rem(ep, NQ)
    half = lax.rem(y, 2)

    def wrap(a, n):
        return lax.rem(a + n, n)

    def at_z(zz):
        return (zz * NQ + q, y)

    def at_q(qq):
        return (z * NQ + qq, y)

    def at_y(yy):
        return (ep, yy)

    def remote(src, dst, ss, rs, dev):
        return pltpu.make_async_remote_copy(src, dst, ss, rs, device_id=dev, device_id_type=MESH)

    barrier = pltpu.get_barrier_semaphore()
    next_ep, prev_ep = wrap(ep + 1, NZ * NQ), wrap(ep - 1, NZ * NQ)
    for i in (1, NZ - 1):
        pl.semaphore_signal(barrier, inc=1, device_id=at_z(wrap(z + i, NZ)), device_id_type=MESH)
    for i in range(1, NQ):
        pl.semaphore_signal(barrier, inc=1, device_id=at_q(wrap(q + i, NQ)), device_id_type=MESH)
    for i in range(1, NY):
        pl.semaphore_signal(barrier, inc=1, device_id=at_y(wrap(y + i, NY)), device_id_type=MESH)
    for e in (next_ep, prev_ep):
        pl.semaphore_signal(barrier, inc=1, device_id=(e, y), device_id_type=MESH)

    own_down = wd_hbm.at[:, pl.ds(pl.multiple_of(y * 1024, 1024), 1024)]
    pairs = (
        (x_hbm, x_ref), (gain_hbm, gain_ref), (rt_hbm, rt_ref), (rw_hbm, rw_ref),
        (k_hbm, k_ref), (v_hbm, v_ref), (q_hbm, q_ref),
        (wg_hbm, W.at[:, :, pl.ds(0, HID)]), (wu_hbm, W.at[:, :, pl.ds(HID, HID)]), (wo_hbm, WO), (own_down, DN.at[y]),
    )
    loads = [pltpu.make_async_copy(src, dst, ls.at[i]) for i, (src, dst) in enumerate(pairs)]
    for load in loads:
        load.start()

    def chunk(j):
        return jnp.where(j < CE, half * CE + j, CE + j)

    loads[0].wait()

    def mean_step(j, total):
        w = x_ref[:, pl.ds(pl.multiple_of(j * 512, 512), 512)].astype(F32)
        return total + jnp.sum(w * w, axis=1, keepdims=True)

    total = lax.fori_loop(0, D // 512, mean_step, jnp.zeros((TOK, 1), F32))
    scale = lax.rsqrt(total * (1.0 / D) + EPS)
    for i in (1, 2, 3):
        loads[i].wait()

    def norm_step(j, _):
        cols = pl.ds(pl.multiple_of(chunk(j) * FC, FC), FC)
        G[j, z] = (x_ref[:, cols].astype(F32) * scale * gain_ref[:, cols]).astype(BF16)
        return 0

    lax.fori_loop(0, C, norm_step, 0)
    IR[z] = jnp.concatenate([rt_ref[...].astype(F32), rw_ref[...]], axis=0)

    def hop(s, d):
        return 6 if s == 3 else 2 * s + d

    def z_copy(j, s, d):
        if d == 0:
            origin, peer = wrap(z - s, NZ), wrap(z + 1, NZ)
        else:
            origin, peer = wrap(z + s, NZ), wrap(z - 1, NZ)
        return remote(G.at[j, origin], G.at[j, origin], zss.at[0], zrs.at[j, hop(s, d)], at_z(peer))

    def i_copy(s, d):
        if d == 0:
            origin, peer = wrap(z - s, NZ), wrap(z + 1, NZ)
        else:
            origin, peer = wrap(z + s, NZ), wrap(z - 1, NZ)
        return remote(IR.at[origin], IR.at[origin], iss.at[0], irs.at[hop(s, d)], at_z(peer))

    def x_copy(j, to):
        return remote(XS.at[j, to], XF.at[j, q], xss.at[0], xrs.at[j], at_q(to))

    def y_copy(j, d):
        to = wrap(y + 1, NY) if d == 0 else wrap(y - 1, NY)
        part = pl.ds(4 * d, 4)
        return remote(XF.at[j, part], XO.at[j, part], yss.at[0], yrs.at[j], at_y(to))

    def d_copy(i):
        to = wrap(y + i, NY)
        src = wd_hbm.at[:, pl.ds(pl.multiple_of(to * 1024, 1024), 1024)]
        return remote(src, DN.at[y], dss.at[0], drs.at[0], at_y(to))

    def a_copy(qq, b, i):
        to = wrap(y + i, NY)
        return remote(ACT.at[y, qq], ACT.at[y, qq], ass.at[0], ars.at[b], at_y(to))

    def w_copy(to):
        return remote(YS.at[to], RX.at[q], wss.at[0], wrs.at[0], at_q(to))

    def s_copy(n, h, d):
        peer = wrap(z + 1, NZ) if d == 0 else wrap(z - 1, NZ)
        return remote(SR.at[n, h], RR.at[n, h], sss.at[0], srs.at[n, h], at_z(peer))

    def m_copy(i):
        to = wrap(y + i, NY)
        return remote(PT.at[to], PM.at[i], mss.at[0], mrs.at[0], at_y(to))

    halo = [
        remote(k_hbm.at[pl.ds(128, 128)], KP.at[0], hss.at[0], hrs.at[0], (next_ep, y)),
        remote(v_hbm.at[pl.ds(128, 128)], KP.at[1], hss.at[0], hrs.at[0], (next_ep, y)),
    ]

    def wait_bytes(view, sem):
        pltpu.make_async_copy(view, view, sem).wait()

    pl.semaphore_wait(barrier, 2 + (NQ - 1) + (NY - 1) + 2)
    for d in range(2):
        z_copy(0, 0, d).start()
        i_copy(0, d).start()
    for j in range(1, AHEAD):
        for d in range(2):
            z_copy(j, 0, d).start()
    for copy in halo:
        copy.start()
    for i in (2, 1, 3):
        d_copy(i).start()
    ACC[...] = jnp.zeros_like(ACC)

    def build_windows():
        wait_bytes(KP, hrs.at[0])
        for i in (4, 5, 6):
            loads[i].wait()
        lanes = lax.broadcasted_iota(jnp.int32, (384, 128), 1)
        for t, (ref, wide) in enumerate(((k_ref, KX), (v_ref, VX))):
            whole = jnp.concatenate([KP[t], ref[...]], axis=0).astype(F32)
            turned = pltpu.roll(whole, 64, 1)
            zero = jnp.zeros_like(whole)
            wide[0, 0] = jnp.where(lanes < 64, whole, zero).astype(BF16)
            wide[1, 1] = jnp.where(lanes < 64, zero, whole).astype(BF16)
            wide[0, 1] = jnp.where(lanes < 64, zero, turned).astype(BF16)
            wide[1, 0] = jnp.where(lanes < 64, turned, zero).astype(BF16)

    def div12(a):
        return (a * 5462) >> 16

    def build_gather():
        u = lax.broadcasted_iota(jnp.int32, (TOK, TOK), 0)
        t = lax.broadcasted_iota(jnp.int32, (TOK, TOK), 1)
        earlier = (u < t).astype(F32).astype(BF16)
        expert = (lax.broadcasted_iota(jnp.int32, (NQ, TOK), 0) + z * NQ).astype(F32)
        named, weight = [], []
        for zs in range(NZ):
            info = IR[zs]
            hits = [(info[k : k + 1, :] == expert).astype(F32) for k in range(4)]
            named.append(hits[0] + hits[1] + hits[2] + hits[3])
            weight.append(sum(hits[k] * info[4 + k : 5 + k, :] for k in range(4)))
        named = jnp.concatenate(named, axis=0)
        rank = jnp.dot(named.astype(BF16), earlier, preferred_element_type=F32)
        rank = jnp.where(named > 0.5, rank, -1.0)
        for zs in range(NZ):
            RANK[zs, 0:8, :] = rank[8 * zs : 8 * zs + 8, :]
            RANK[zs, 8:16, :] = weight[zs]
        row = lax.broadcasted_iota(jnp.int32, (ROWS, 128), 0)
        row_z = div12(row)
        row_k = (row - row_z * CAP).astype(F32)

        def step(zs, _):
            cols = pl.ds(pl.multiple_of(zs * TOK, TOK), TOK)
            ranks = RANK[zs, 0:8, :]
            for e in range(NQ):
                hit = (row_z == zs) & (ranks[e : e + 1, :] == row_k)
                S[e, :, cols] = hit.astype(F32).astype(BF16)
            return 0

        lax.fori_loop(0, NZ, step, 0)

    def build_combine():
        i16 = lax.broadcasted_iota(jnp.int32, (16, NQ * ROWS), 0)
        col = lax.broadcasted_iota(jnp.int32, (16, NQ * ROWS), 1)
        col_q = (div12(col)) >> 3
        spread_rank = (i16 == col_q).astype(F32).astype(BF16)
        spread_weight = (i16 == col_q + 8).astype(F32).astype(BF16)
        col = lax.broadcasted_iota(jnp.int32, (TOK, NQ * ROWS), 1)
        col12 = div12(col)
        col_z = col12 & 7
        col_k = (col - col12 * CAP).astype(F32)

        def step(zs, _):
            turned = RANK[zs].T.astype(BF16)
            ranks = jnp.dot(turned, spread_rank, preferred_element_type=F32)
            weights = jnp.dot(turned, spread_weight, preferred_element_type=F32)
            hit = (col_z == zs) & (ranks == col_k)
            CM[zs] = jnp.where(hit, weights, 0.0).astype(BF16)
            return 0

        lax.fori_loop(0, NZ, step, 0)

    def attend(u):
        n, p = u // 4, lax.rem(u, 4)
        kv = p // 2
        rows = pl.ds(pl.multiple_of(n * 128, 128), 128)
        window = pl.ds(pl.multiple_of(n * 128, 128), 256)
        cols = pl.ds(pl.multiple_of(p * 128, 128), 128)
        queries = q_ref[rows, cols]
        i = lax.broadcasted_iota(jnp.int32, (128, 256), 0)
        s = lax.broadcasted_iota(jnp.int32, (128, 256), 1)
        first = jnp.where((ep == 0) & (n == 0), 128, 0)
        seen = (s > i) & (s <= i + 128) & (s >= first)
        both = jnp.zeros((128, 128), F32)
        for h in range(2):
            scores = lax.dot_general(
                queries, KX[kv, h, window, :], (((1,), (1,)), ((), ())), preferred_element_type=F32
            ) * 0.125
            scores = jnp.where(seen, scores, -jnp.inf)
            sink = sink_ref[2 * p + h]
            highest = jnp.maximum(jnp.max(scores, axis=1, keepdims=True), sink)
            e = jnp.exp(scores - highest)
            under = jnp.sum(e, axis=1, keepdims=True) + jnp.exp(sink - highest)
            w = (e / under).astype(BF16)
            both = both + jnp.dot(w, VX[kv, h, window, :], preferred_element_type=F32)
        ATT[rows, cols] = both.astype(BF16)

    def project(u):
        cols = pl.ds(pl.multiple_of(u * 512, 512), 512)
        part = jnp.dot(ATT[...], WO[:, cols], preferred_element_type=F32).astype(BF16)
        PT[:, :, cols] = part.reshape(NY, 64, 512)

    def expert_dots(*terms):
        def step(r, _):
            part = pl.ds(4 * r, 4)
            rows = pl.ds(pl.multiple_of(r * 4 * ROWS, 4 * ROWS), 4 * ROWS)
            value = ACC[rows, :]
            for src, j, w in terms:
                block = src[j, part].reshape(4 * ROWS, FC)
                value = value + jnp.dot(block, W[w], preferred_element_type=F32)
            ACC[rows, :] = value
            return 0

        lax.fori_loop(0, 2, step, 0)

    def within(j):
        return (j >= 0) & (j < C)

    def tick(t, _):
        @pl.when(within(t - 3))
        def _():
            j = t - 3

            @pl.when(j == 0)
            def _():
                i_copy(2, 0).wait_recv()
                i_copy(2, 1).wait_recv()
                i_copy(3, 0).start()

            for d in range(2):
                z_copy(j, 2, d).wait_recv()

                @pl.when(lax.rem(j, 2) == d)
                def _():
                    z_copy(j, 3, d).start()

        for s in (2, 1):

            @pl.when(within(t - s))
            def _():
                for d in range(2):

                    @pl.when(t == s)
                    def _():
                        i_copy(s - 1, d).wait_recv()
                        i_copy(s, d).start()

                    z_copy(t - s, s - 1, d).wait_recv()
                    z_copy(t - s, s, d).start()

        @pl.when(t + AHEAD < C)
        def _():
            for d in range(2):
                z_copy(t + AHEAD, 0, d).start()

        @pl.when(within(t - 4))
        def _():
            j = t - 4

            @pl.when(j == 0)
            def _():
                i_copy(3, 0).wait_recv()
                build_gather()

            for d in range(2):

                @pl.when(lax.rem(j, 2) == d)
                def _():
                    z_copy(j, 3, d).wait_recv()

            def step(r, _):
                part = pl.ds(4 * r, 4)
                block = jnp.dot(
                    S[part].reshape(4 * ROWS, NZ * TOK), G[j].reshape(NZ * TOK, FC), preferred_element_type=F32
                ).astype(BF16)
                XS[j, part] = block.reshape(4, ROWS, FC)
                for i in range(4):

                    @pl.when(4 * r + i != q)
                    def _():
                        x_copy(j, 4 * r + i).start()

                return 0

            lax.fori_loop(0, 2, step, 0)
            XF[j, q] = XS[j, q]

        @pl.when(within(t - 6))
        def _():
            j = t - 6
            wait_bytes(XF.at[j, pl.ds(0, NQ - 1)], xrs.at[j])

            @pl.when(j < CE)
            def _():
                for d in range(2):
                    y_copy(j, d).start()

            @pl.when(j == 0)
            def _():
                loads[7].wait()
                loads[8].wait()

        @pl.when((t >= 6) & (t < 8))
        def _():
            expert_dots((XF, t - 6, chunk(t - 6)))

        @pl.when((t >= 8) & (t < 8 + CE))
        def _():
            j = t - 8
            wait_bytes(XO.at[j], yrs.at[j])
            expert_dots((XF, t - 6, chunk(t - 6)), (XO, j, (1 - half) * CE + j))

        @pl.when(t == 2)
        def _():
            build_windows()

        @pl.when((t >= 3) & (t < 7))
        def _():
            for i in range(2):
                attend((t - 3) * 2 + i)

        return 0

    lax.fori_loop(0, C + 6, tick, 0)

    def pair(b):
        chip, core = q // 2, lax.rem(q, 2)
        apart = (b > 0) & (b < 3)
        dx = jnp.where(b == 0, 2, jnp.where(b == 3, 0, 1))
        dc = jnp.where(apart, b - 1, 0)
        first = lax.rem(chip + dx, 4) * 2 + lax.rem(core + dc, 2)
        dx = jnp.where(apart, 3, dx)
        dc = jnp.where(apart, b - 1, 1)
        return first, lax.rem(chip + dx, 4) * 2 + lax.rem(core + dc, 2)

    def activate(b, _):
        for qq in pair(b):
            rows = pl.ds(pl.multiple_of(qq * ROWS, ROWS), ROWS)
            g = jnp.minimum(ACC[rows, 0:HID], CLAMP)
            u = jnp.clip(ACC[rows, HID : 2 * HID], -CLAMP, CLAMP) + 1.0
            ACT[y, qq] = (u * g * jax.nn.sigmoid(SLOPE * g)).astype(BF16)
            for i in (2, 1, 3):
                a_copy(qq, b, i).start()
        return 0

    lax.fori_loop(0, 4, activate, 0)
    build_combine()
    loads[9].wait()

    def project_step(u, _):
        project(u)
        return 0

    lax.fori_loop(0, D // 512, project_step, 0)
    loads[10].wait()
    wait_bytes(DN.at[pl.ds(0, NY - 1)], drs.at[0])

    def down(b, _):
        wait_bytes(ACT.at[pl.ds(0, NY - 1), pl.ds(0, 2)], ars.at[b])

        @pl.when(b == 3)
        def _():
            for i in (2, 1, 3):
                m_copy(i).start()

        qs = pair(b)
        block = jnp.zeros((2 * ROWS, 1024), F32)
        for i in range(NY):
            acts = jnp.concatenate([ACT[i, qq] for qq in qs], axis=0)
            block = block + jnp.dot(acts, DN[i], preferred_element_type=F32)
        for i, qq in enumerate(qs):
            YS[qq] = block[i * ROWS : (i + 1) * ROWS].astype(BF16)

            @pl.when(qq != q)
            def _():
                w_copy(qq).start()

        return 0

    lax.fori_loop(0, 4, down, 0)
    RX[q] = YS[q]
    wait_bytes(RX.at[pl.ds(0, NQ - 1)], wrs.at[0])

    def partial_sum(n, zd):
        cols = pl.ds(pl.multiple_of(n * FC, FC), FC)
        return jnp.dot(CM[zd], RX[:, :, cols].reshape(NQ * ROWS, FC), preferred_element_type=F32)

    def send_sum(n, s, d):
        odd = lax.rem(n, 2)
        ahead = (4 - odd if d == 0 else 3 + odd) - s
        zd = wrap(z + ahead, NZ) if d == 0 else wrap(z - ahead, NZ)
        value = partial_sum(n, zd)
        if s > 0:
            before = hop(s - 1, d)
            s_copy(n, before, d).wait_recv()
            value = value + RR[n, before].astype(F32)
        SR[n, hop(s, d)] = value.astype(BF16)
        s_copy(n, hop(s, d), d).start()

    for s in range(4):

        def send_step(n, _):
            for d in range(2):
                if s < 3:
                    send_sum(n, s, d)
                else:

                    @pl.when(lax.rem(n, 2) == d)
                    def _():
                        send_sum(n, s, d)

            return 0

        lax.fori_loop(0, NB, send_step, 0)

    def finish(n, _):
        odd = lax.rem(n, 2)
        value = partial_sum(n, z)
        for d in range(2):
            last = jnp.where(odd == d, 6, 4 + d)
            s_copy(n, last, d).wait_recv()
            value = value + RR[n, last].astype(F32)
        out_ref[:, pl.ds(pl.multiple_of(n * FC, FC), FC)] = value.astype(BF16)
        return 0

    lax.fori_loop(0, NB, finish, 0)

    wait_bytes(PM.at[pl.ds(1, NY - 1)], mrs.at[0])

    def mix(u, _):
        cols = pl.ds(pl.multiple_of(u * 512, 512), 512)
        value = PT[y, :, cols].astype(F32)
        for i in range(1, NY):
            value = value + PM[i, :, cols].astype(F32)
        mix_ref[:, cols] = value.astype(BF16)
        return 0

    lax.fori_loop(0, D // 512, mix, 0)

    for view, sem in (
        (G.at[:, pl.ds(0, 7)], zss),
        (IR.at[pl.ds(0, 7)], iss),
        (XS.at[:, pl.ds(0, NQ - 1)], xss),
        (XO, yss),
        (DN.at[pl.ds(0, NY - 1)], dss),
        (ACT.at[pl.ds(0, NY - 1)], ass),
        (RX.at[pl.ds(0, NQ - 1)], wss),
        (SR, sss),
        (PM.at[pl.ds(1, NY - 1)], mss),
        (KP, hss),
    ):
        wait_bytes(view, sem.at[0])


def write_out(mix_in, out_in, mix_ref, out_ref):
    mix_ref[...] = mix_in[...]
    out_ref[...] = out_in[...]


def shards(
    projected_queries,
    key_proj,
    projected_values,
    head_sink_logits,
    out_weight,
    expert_input,
    norm_gain,
    routing,
    route_weight,
    gate_weight,
    up_weight,
    down_weight,
):
    vmem = pl.BlockSpec(memory_space=pltpu.VMEM)
    hbm = pl.BlockSpec(memory_space=pl.ANY)
    smem = pl.BlockSpec(memory_space=pltpu.SMEM)
    dma = pltpu.SemaphoreType.DMA
    mixed, combined = pl.pallas_call(
        kernel,
        out_shape=(
            jax.ShapeDtypeStruct((64, D), BF16),
            jax.ShapeDtypeStruct((TOK, 1024), BF16),
        ),
        in_specs=[hbm, hbm, hbm, smem, hbm, hbm, hbm, hbm, hbm, hbm, hbm, hbm],
        out_specs=(vmem, vmem),
        scratch_shapes=[
            pltpu.VMEM((256, 512), BF16),
            pltpu.VMEM((256, 128), BF16),
            pltpu.VMEM((256, 128), BF16),
            pltpu.VMEM((TOK, D), BF16),
            pltpu.VMEM((1, D), F32),
            pltpu.VMEM((4, TOK), jnp.int32),
            pltpu.VMEM((4, TOK), F32),
            pltpu.VMEM((C, NZ, TOK, FC), BF16),
            pltpu.VMEM((C, NQ, ROWS, FC), BF16),
            pltpu.VMEM((C, NQ, ROWS, FC), BF16),
            pltpu.VMEM((CE, NQ, ROWS, FC), BF16),
            pltpu.VMEM((D // FC, FC, 2 * HID), BF16),
            pltpu.VMEM((512, D), BF16),
            pltpu.VMEM((NY, HID, 1024), BF16),
            pltpu.VMEM((NQ, ROWS, NZ * TOK), BF16),
            pltpu.VMEM((NZ, TOK, NQ * ROWS), BF16),
            pltpu.VMEM((NZ, 8, TOK), F32),
            pltpu.VMEM((NZ, 16, TOK), F32),
            pltpu.VMEM((NQ * ROWS, 2 * HID), F32),
            pltpu.VMEM((NY, NQ, ROWS, HID), BF16),
            pltpu.VMEM((NQ, ROWS, 1024), BF16),
            pltpu.VMEM((NQ, ROWS, 1024), BF16),
            pltpu.VMEM((NB, 7, TOK, FC), BF16),
            pltpu.VMEM((NB, 7, TOK, FC), BF16),
            pltpu.VMEM((2, 128, 128), BF16),
            pltpu.VMEM((2, 2, 384, 128), BF16),
            pltpu.VMEM((2, 2, 384, 128), BF16),
            pltpu.VMEM((256, 512), BF16),
            pltpu.VMEM((NY, 64, D), BF16),
            pltpu.VMEM((NY, 64, D), BF16),
            dma((11,)),
            dma((1,)), dma((C, 7)),
            dma((1,)), dma((7,)),
            dma((1,)), dma((C,)),
            dma((1,)), dma((CE,)),
            dma((1,)), dma((1,)),
            dma((1,)), dma((4,)),
            dma((1,)), dma((1,)),
            dma((1,)), dma((NB, 7)),
            dma((1,)), dma((1,)),
            dma((1,)), dma((1,)),
        ],
        compiler_params=pltpu.CompilerParams(
            collective_id=0, has_side_effects=True, vmem_limit_bytes=62 * 1024 * 1024
        ),
    )(
        projected_queries,
        key_proj,
        projected_values,
        head_sink_logits,
        out_weight,
        expert_input,
        norm_gain.reshape(1, D),
        routing.T,
        route_weight.T,
        gate_weight.reshape(D // FC, FC, HID),
        up_weight.reshape(D // FC, FC, HID),
        down_weight.reshape(HID, D),
    )
    return pl.pallas_call(
        write_out,
        out_shape=(
            jax.ShapeDtypeStruct((64, D), BF16),
            jax.ShapeDtypeStruct((TOK, 1024), BF16),
        ),
        in_specs=[vmem, vmem],
        out_specs=(vmem, vmem),
    )(mixed, combined)


def solution(mesh):
    placed = (
        P("ep", "tp"),
        P("ep", "tp"),
        P("ep", "tp"),
        P("tp"),
        P("tp", None),
        P("ep", None),
        P(),
        P("ep", None),
        P("ep", None),
        P("ep", None, "tp"),
        P("ep", None, "tp"),
        P("ep", "tp", None),
    )
    return jax.shard_map(
        shards,
        mesh=mesh,
        in_specs=placed,
        out_specs=(P(("ep", "tp"), None), P("ep", "tp")),
        check_vma=False,
    )
```

time: 161 us -> 129 us (0.80)
  Pallas kernels: 152 us -> 127 us
  local copies, waits for them, and re-layouts: 6.37 us -> 0 us
    pallas_call x1, Pallas kernels: 152 us -> 125 us  [shards(): pl.pallas_call(kernel, out_shape=(jax.ShapeDtypeStruct((64, D), BF16), ja...]
    unnamed x4 -> x0, local copies, waits for them, and re-layouts: 6.37 us -> none
    pallas_call x0 -> x1, Pallas kernels: none -> 2.02 us  [shards(): pl.pallas_call(write_out, out_shape=(jax.ShapeDtypeStruct((64, D), BF16),...]
where the time goes in v2:
time: 129 us; the launch traced here: 128 us
  Pallas kernels  127 us (98%)
    pallas_call x1, Pallas kernels, shards(): pl.pallas_call(kernel, out_shape=(jax.ShapeDtypeStruct((64, D), BF16), ja...  125 us

profile of v2, /device:TPU:2, one launch (start us, length us, event | category | flops | bytes accessed | tf_op | source)
XLA Modules:
  0.0 128.0 jit_solution(777221209448341012)
XLA Ops:
  0.6 125.3 %shard_map.131 = (bf16[64,4096]{1,0:T(8,128)(2,1)}, bf16[128,1024]{1,0:T(8,128)(2,1)}) custom-call(bf16[256,512]{1,0:T(8,128)(2,1)} %q_hbm.1, bf16[256,128]{1,0:T(8,128)(2,1)} %k_hbm.1, bf16[256,128]{1,0:T(8,128)(2,1)} %v_hbm.1, f32[8]{0:T(128)} %sink_ref.1, bf16[512,4096]{1,0:T(8,128)(2,1)} %wo_hbm.1, bf16[128,4096]{1,0:T(8,128)(2,1)} %x_hbm.1, ...), custom_call_target="tpu_custom_call" | custom-call | tf_op jit(solution)/shard_map/pallas_call | solution.py:542
  126.0 2.0 %shard_map.132 = (bf16[64,4096]{1,0:T(8,128)(2,1)}, bf16[128,1024]{1,0:T(8,128)(2,1)}) custom-call(bf16[64,4096]{1,0:T(8,128)(2,1)} %get-tuple-element.4.mix_in, bf16[128,1024]{1,0:T(8,128)(2,1)} %get-tuple-element.5.out_in), custom_call_target="tpu_custom_call" | custom-call | tf_op jit(solution)/shard_map/pallas_call | solution.py:610

commit v3 on v2

--- a/solution.py
+++ b/solution.py
@@ -19,9 +19,12 @@
 FC = 256
 CE = 7
 C = 9
-AHEAD = 2
+AHEAD = 3
 HID = 256
 NB = 4
+HALF = ROWS // 2
+PLACE = (7, 5, 3, 1, 0, 2, 4, 6)
+OWN = 7
 MESH = pl.DeviceIdType.MESH
 F32 = jnp.float32
 BF16 = jnp.bfloat16
@@ -32,7 +35,7 @@
     mix_ref, out_ref,
     q_ref, k_ref, v_ref, x_ref, gain_ref, rt_ref, rw_ref,
     G, XS, XF, XO, W, WO, DN, S, CM, IR, RANK, ACC, ACT, YS, RX, SR, RR,
-    KP, KX, VX, ATT, PT, PM,
+    KP, KX, VX, ATT, PT, PM, PN,
     ls, zss, zrs, iss, irs, xss, xrs, yss, yrs, dss, drs, ass, ars, wss, wrs, sss, srs, mss, mrs, hss, hrs,
 ):
     ep = lax.axis_index("ep")
@@ -84,37 +87,37 @@
 
     def mean_step(j, total):
         w = x_ref[:, pl.ds(pl.multiple_of(j * 512, 512), 512)].astype(F32)
-        return total + jnp.sum(w * w, axis=1, keepdims=True)
-
-    total = lax.fori_loop(0, D // 512, mean_step, jnp.zeros((TOK, 1), F32))
-    scale = lax.rsqrt(total * (1.0 / D) + EPS)
+        w = w * w
+        return total + ((w[:, 0:128] + w[:, 128:256]) + (w[:, 256:384] + w[:, 384:512]))
+
+    total = lax.fori_loop(0, D // 512, mean_step, jnp.zeros((TOK, 128), F32))
+    scale = lax.rsqrt(jnp.sum(total, axis=1, keepdims=True) * (1.0 / D) + EPS)
     for i in (1, 2, 3):
         loads[i].wait()
 
     def norm_step(j, _):
         cols = pl.ds(pl.multiple_of(chunk(j) * FC, FC), FC)
-        G[j, z] = (x_ref[:, cols].astype(F32) * scale * gain_ref[:, cols]).astype(BF16)
+        G[j, OWN] = (x_ref[:, cols].astype(F32) * scale * gain_ref[:, cols]).astype(BF16)
         return 0
 
     lax.fori_loop(0, C, norm_step, 0)
-    IR[z] = jnp.concatenate([rt_ref[...].astype(F32), rw_ref[...]], axis=0)
+    IR[OWN] = jnp.concatenate([rt_ref[...].astype(F32), rw_ref[...]], axis=0)
 
     def hop(s, d):
         return 6 if s == 3 else 2 * s + d
 
+    def ring(s, d):
+        if d == 0:
+            return PLACE[-s % NZ], PLACE[-(s + 1) % NZ], at_z(wrap(z + 1, NZ))
+        return PLACE[s], PLACE[s + 1], at_z(wrap(z - 1, NZ))
+
     def z_copy(j, s, d):
-        if d == 0:
-            origin, peer = wrap(z - s, NZ), wrap(z + 1, NZ)
-        else:
-            origin, peer = wrap(z + s, NZ), wrap(z - 1, NZ)
-        return remote(G.at[j, origin], G.at[j, origin], zss.at[0], zrs.at[j, hop(s, d)], at_z(peer))
+        here, there, to = ring(s, d)
+        return remote(G.at[j, here], G.at[j, there], zss.at[0], zrs.at[j, hop(s, d)], to)
 
     def i_copy(s, d):
-        if d == 0:
-            origin, peer = wrap(z - s, NZ), wrap(z + 1, NZ)
-        else:
-            origin, peer = wrap(z + s, NZ), wrap(z - 1, NZ)
-        return remote(IR.at[origin], IR.at[origin], iss.at[0], irs.at[hop(s, d)], at_z(peer))
+        here, there, to = ring(s, d)
+        return remote(IR.at[here], IR.at[there], iss.at[0], irs.at[hop(s, d)], to)
 
     def x_copy(j, to):
         return remote(XS.at[j, to], XF.at[j, q], xss.at[0], xrs.at[j], at_q(to))
@@ -129,20 +132,22 @@
         src = wd_hbm.at[:, pl.ds(pl.multiple_of(to * 1024, 1024), 1024)]
         return remote(src, DN.at[y], dss.at[0], drs.at[0], at_y(to))
 
-    def a_copy(qq, b, i):
+    def a_copy(h, qq, b, i):
         to = wrap(y + i, NY)
-        return remote(ACT.at[y, qq], ACT.at[y, qq], ass.at[0], ars.at[b], at_y(to))
-
-    def w_copy(to):
-        return remote(YS.at[to], RX.at[q], wss.at[0], wrs.at[0], at_q(to))
+        return remote(ACT.at[y, h, qq], ACT.at[y, h, qq], ass.at[0], ars.at[4 * h + b], at_y(to))
+
+    def w_copy(h, to):
+        return remote(YS.at[h, to], RX.at[h, q], wss.at[0], wrs.at[h], at_q(to))
 
     def s_copy(n, h, d):
         peer = wrap(z + 1, NZ) if d == 0 else wrap(z - 1, NZ)
         return remote(SR.at[n, h], RR.at[n, h], sss.at[0], srs.at[n, h], at_z(peer))
 
-    def m_copy(i):
-        to = wrap(y + i, NY)
-        return remote(PT.at[to], PM.at[i], mss.at[0], mrs.at[0], at_y(to))
+    def m_copy(step, d):
+        to = wrap(y + 1, NY) if d == 0 else wrap(y - 1, NY)
+        if step == 0:
+            return remote(PT.at[wrap(y + 2, NY), d], PM.at[d], mss.at[0], mrs.at[d], at_y(to))
+        return remote(PT.at[to], PN.at[d], mss.at[1], mrs.at[2 + d], at_y(to))
 
     halo = [
         remote(k_hbm.at[pl.ds(128, 128)], KP.at[0], hss.at[0], hrs.at[0], (next_ep, y)),
@@ -165,19 +170,26 @@
         d_copy(i).start()
     ACC[...] = jnp.zeros_like(ACC)
 
-    def build_windows():
-        wait_bytes(KP, hrs.at[0])
+    def widen(whole, wide, rows):
+        lanes = lax.broadcasted_iota(jnp.int32, whole.shape, 1)
+        whole = whole.astype(F32)
+        turned = pltpu.roll(whole, 64, 1)
+        zero = jnp.zeros_like(whole)
+        wide[0, 0, rows, :] = jnp.where(lanes < 64, whole, zero).astype(BF16)
+        wide[1, 1, rows, :] = jnp.where(lanes < 64, zero, whole).astype(BF16)
+        wide[0, 1, rows, :] = jnp.where(lanes < 64, zero, turned).astype(BF16)
+        wide[1, 0, rows, :] = jnp.where(lanes < 64, turned, zero).astype(BF16)
+
+    def own_windows():
         for i in (4, 5, 6):
             loads[i].wait()
-        lanes = lax.broadcasted_iota(jnp.int32, (384, 128), 1)
-        for t, (ref, wide) in enumerate(((k_ref, KX), (v_ref, VX))):
-            whole = jnp.concatenate([KP[t], ref[...]], axis=0).astype(F32)
-            turned = pltpu.roll(whole, 64, 1)
-            zero = jnp.zeros_like(whole)
-            wide[0, 0] = jnp.where(lanes < 64, whole, zero).astype(BF16)
-            wide[1, 1] = jnp.where(lanes < 64, zero, whole).astype(BF16)
-            wide[0, 1] = jnp.where(lanes < 64, zero, turned).astype(BF16)
-            wide[1, 0] = jnp.where(lanes < 64, turned, zero).astype(BF16)
+        widen(k_ref[...], KX, pl.ds(128, 256))
+        widen(v_ref[...], VX, pl.ds(128, 256))
+
+    def prior_windows():
+        wait_bytes(KP, hrs.at[0])
+        widen(KP[0], KX, pl.ds(0, 128))
+        widen(KP[1], VX, pl.ds(0, 128))
 
     def div12(a):
         return (a * 5462) >> 16
@@ -200,36 +212,35 @@
             RANK[zs, 0:8, :] = rank[8 * zs : 8 * zs + 8, :]
             RANK[zs, 8:16, :] = weight[zs]
         row = lax.broadcasted_iota(jnp.int32, (ROWS, 128), 0)
-        row_z = div12(row)
-        row_k = (row - row_z * CAP).astype(F32)
+        row_p = div12(row)
+        row_k = (row - row_p * CAP).astype(F32)
 
         def step(zs, _):
             cols = pl.ds(pl.multiple_of(zs * TOK, TOK), TOK)
             ranks = RANK[zs, 0:8, :]
             for e in range(NQ):
-                hit = (row_z == zs) & (ranks[e : e + 1, :] == row_k)
+                hit = (row_p == zs) & (ranks[e : e + 1, :] == row_k)
                 S[e, :, cols] = hit.astype(F32).astype(BF16)
             return 0
 
         lax.fori_loop(0, NZ, step, 0)
 
     def build_combine():
-        i16 = lax.broadcasted_iota(jnp.int32, (16, NQ * ROWS), 0)
-        col = lax.broadcasted_iota(jnp.int32, (16, NQ * ROWS), 1)
-        col_q = (div12(col)) >> 3
+        i16 = lax.broadcasted_iota(jnp.int32, (16, NQ * HALF), 0)
+        col_q = div12(lax.broadcasted_iota(jnp.int32, (16, NQ * HALF), 1)) >> 2
         spread_rank = (i16 == col_q).astype(F32).astype(BF16)
         spread_weight = (i16 == col_q + 8).astype(F32).astype(BF16)
-        col = lax.broadcasted_iota(jnp.int32, (TOK, NQ * ROWS), 1)
+        col = lax.broadcasted_iota(jnp.int32, (TOK, NQ * HALF), 1)
         col12 = div12(col)
-        col_z = col12 & 7
+        col_p = col12 & 3
         col_k = (col - col12 * CAP).astype(F32)
 
-        def step(zs, _):
-            turned = RANK[zs].T.astype(BF16)
+        def step(p, _):
+            turned = RANK[p].T.astype(BF16)
             ranks = jnp.dot(turned, spread_rank, preferred_element_type=F32)
             weights = jnp.dot(turned, spread_weight, preferred_element_type=F32)
-            hit = (col_z == zs) & (ranks == col_k)
-            CM[zs] = jnp.where(hit, weights, 0.0).astype(BF16)
+            hit = (col_p == (p & 3)) & (ranks == col_k)
+            CM[p] = jnp.where(hit, weights, 0.0).astype(BF16)
             return 0
 
         lax.fori_loop(0, NZ, step, 0)
@@ -262,7 +273,8 @@
     def project(u):
         cols = pl.ds(pl.multiple_of(u * 512, 512), 512)
         part = jnp.dot(ATT[...], WO[:, cols], preferred_element_type=F32).astype(BF16)
-        PT[:, :, cols] = part.reshape(NY, 64, 512)
+        inner = pl.ds(pl.multiple_of(lax.rem(u, 4) * 512, 512), 512)
+        PT[:, u // 4, :, inner] = part.reshape(NY, 64, 512)
 
     def expert_dots(*terms):
         def step(r, _):
@@ -280,6 +292,18 @@
     def within(j):
         return (j >= 0) & (j < C)
 
+    def pick(j, r):
+        part = pl.ds(4 * r, 4)
+        block = jnp.dot(
+            S[part].reshape(4 * ROWS, NZ * TOK), G[j].reshape(NZ * TOK, FC), preferred_element_type=F32
+        ).astype(BF16)
+        XS[j, part] = block.reshape(4, ROWS, FC)
+        for i in range(4):
+
+            @pl.when(4 * r + i != q)
+            def _():
+                x_copy(j, 4 * r + i).start()
+
     def tick(t, _):
         @pl.when(within(t - 3))
         def _():
@@ -297,6 +321,23 @@
                 @pl.when(lax.rem(j, 2) == d)
                 def _():
                     z_copy(j, 3, d).start()
+
+        @pl.when(within(t - 4))
+        def _():
+            j = t - 4
+
+            @pl.when(j == 0)
+            def _():
+                i_copy(3, 0).wait_recv()
+                build_gather()
+
+            for d in range(2):
+
+                @pl.when(lax.rem(j, 2) == d)
+                def _():
+                    z_copy(j, 3, d).wait_recv()
+
+            pick(j, 0)
 
         for s in (2, 1):
 
@@ -312,42 +353,22 @@
                     z_copy(t - s, s - 1, d).wait_recv()
                     z_copy(t - s, s, d).start()
 
-        @pl.when(t + AHEAD < C)
+            if s == 2:
+
+                @pl.when(within(t - 4))
+                def _():
+                    pick(t - 4, 1)
+                    XF[t - 4, q] = XS[t - 4, q]
+
+        @pl.when(t == 1)
+        def _():
+            for d in range(2):
+                z_copy(AHEAD, 0, d).start()
+
+        @pl.when((t > 0) & (t + AHEAD < C))
         def _():
             for d in range(2):
                 z_copy(t + AHEAD, 0, d).start()
-
-        @pl.when(within(t - 4))
-        def _():
-            j = t - 4
-
-            @pl.when(j == 0)
-            def _():
-                i_copy(3, 0).wait_recv()
-                build_gather()
-
-            for d in range(2):
-
-                @pl.when(lax.rem(j, 2) == d)
-                def _():
-                    z_copy(j, 3, d).wait_recv()
-
-            def step(r, _):
-                part = pl.ds(4 * r, 4)
-                block = jnp.dot(
-                    S[part].reshape(4 * ROWS, NZ * TOK), G[j].reshape(NZ * TOK, FC), preferred_element_type=F32
-                ).astype(BF16)
-                XS[j, part] = block.reshape(4, ROWS, FC)
-                for i in range(4):
-
-                    @pl.when(4 * r + i != q)
-                    def _():
-                        x_copy(j, 4 * r + i).start()
-
-                return 0
-
-            lax.fori_loop(0, 2, step, 0)
-            XF[j, q] = XS[j, q]
 
         @pl.when(within(t - 6))
         def _():
@@ -374,14 +395,32 @@
             wait_bytes(XO.at[j], yrs.at[j])
             expert_dots((XF, t - 6, chunk(t - 6)), (XO, j, (1 - half) * CE + j))
 
+        @pl.when(t == 0)
+        def _():
+            own_windows()
+
         @pl.when(t == 2)
         def _():
-            build_windows()
-
-        @pl.when((t >= 3) & (t < 7))
-        def _():
-            for i in range(2):
-                attend((t - 3) * 2 + i)
+            prior_windows()
+
+        @pl.when((t == 1) | (t == 2))
+        def _():
+            for i in range(4):
+                attend((2 - t) * 4 + i)
+
+        @pl.when(t == 3)
+        def _():
+            loads[9].wait()
+
+        @pl.when((t == 3) | (t == 4))
+        def _():
+            for i in range(4):
+                project((t - 3) * 4 + i)
+
+        @pl.when(t == 4)
+        def _():
+            for d in range(2):
+                m_copy(0, d).start()
 
         return 0
 
@@ -397,63 +436,64 @@
         dc = jnp.where(apart, b - 1, 1)
         return first, lax.rem(chip + dx, 4) * 2 + lax.rem(core + dc, 2)
 
-    def activate(b, _):
+    def activate(hb, _):
+        h, b = hb // 4, lax.rem(hb, 4)
         for qq in pair(b):
-            rows = pl.ds(pl.multiple_of(qq * ROWS, ROWS), ROWS)
+            rows = pl.ds(pl.multiple_of(qq * ROWS + h * HALF, 16), HALF)
             g = jnp.minimum(ACC[rows, 0:HID], CLAMP)
             u = jnp.clip(ACC[rows, HID : 2 * HID], -CLAMP, CLAMP) + 1.0
-            ACT[y, qq] = (u * g * jax.nn.sigmoid(SLOPE * g)).astype(BF16)
+            ACT[y, h, qq] = (u * g * jax.nn.sigmoid(SLOPE * g)).astype(BF16)
             for i in (2, 1, 3):
-                a_copy(qq, b, i).start()
+                a_copy(h, qq, b, i).start()
         return 0
 
-    lax.fori_loop(0, 4, activate, 0)
+    lax.fori_loop(0, 8, activate, 0)
     build_combine()
-    loads[9].wait()
-
-    def project_step(u, _):
-        project(u)
-        return 0
-
-    lax.fori_loop(0, D // 512, project_step, 0)
     loads[10].wait()
     wait_bytes(DN.at[pl.ds(0, NY - 1)], drs.at[0])
-
-    def down(b, _):
-        wait_bytes(ACT.at[pl.ds(0, NY - 1), pl.ds(0, 2)], ars.at[b])
-
-        @pl.when(b == 3)
-        def _():
-            for i in (2, 1, 3):
-                m_copy(i).start()
-
+    for d in range(2):
+        wait_bytes(PM.at[d], mrs.at[d])
+        to = wrap(y + 1, NY) if d == 0 else wrap(y - 1, NY)
+        PT[to, d] = (PT[to, d].astype(F32) + PM[d].astype(F32)).astype(BF16)
+
+    def down(hb, _):
+        h, b = hb // 4, lax.rem(hb, 4)
+        wait_bytes(ACT.at[pl.ds(0, NY - 1), 0, pl.ds(0, 2)], ars.at[hb])
         qs = pair(b)
-        block = jnp.zeros((2 * ROWS, 1024), F32)
+        block = jnp.zeros((2 * HALF, 1024), F32)
         for i in range(NY):
-            acts = jnp.concatenate([ACT[i, qq] for qq in qs], axis=0)
+            acts = jnp.concatenate([ACT[i, h, qq] for qq in qs], axis=0)
             block = block + jnp.dot(acts, DN[i], preferred_element_type=F32)
         for i, qq in enumerate(qs):
-            YS[qq] = block[i * ROWS : (i + 1) * ROWS].astype(BF16)
+            YS[h, qq] = block[i * HALF : (i + 1) * HALF].astype(BF16)
 
             @pl.when(qq != q)
             def _():
-                w_copy(qq).start()
+                w_copy(h, qq).start()
+
+            @pl.when(qq == q)
+            def _():
+                RX[h, q] = YS[h, q]
 
         return 0
 
-    lax.fori_loop(0, 4, down, 0)
-    RX[q] = YS[q]
-    wait_bytes(RX.at[pl.ds(0, NQ - 1)], wrs.at[0])
-
-    def partial_sum(n, zd):
+    lax.fori_loop(0, 6, down, 0)
+    wait_bytes(RX.at[0, pl.ds(0, NQ - 1)], wrs.at[0])
+
+    def partial_sum(n, place):
         cols = pl.ds(pl.multiple_of(n * FC, FC), FC)
-        return jnp.dot(CM[zd], RX[:, :, cols].reshape(NQ * ROWS, FC), preferred_element_type=F32)
+        rows = RX[place // 4, :, :, cols].reshape(NQ * HALF, FC)
+        return jnp.dot(CM[place], rows, preferred_element_type=F32)
 
     def send_sum(n, s, d):
         odd = lax.rem(n, 2)
-        ahead = (4 - odd if d == 0 else 3 + odd) - s
-        zd = wrap(z + ahead, NZ) if d == 0 else wrap(z - ahead, NZ)
-        value = partial_sum(n, zd)
+        if d == 0:
+            ahead = 4 - odd - s
+            place = jnp.where(ahead == 4, 0, 2 * (4 - ahead) - 1)
+        else:
+            ahead = 3 + odd - s
+            place = 2 * (4 - ahead)
+        value = partial_sum(n, place)
         if s > 0:
             before = hop(s - 1, d)
             s_copy(n, before, d).wait_recv()
@@ -461,45 +501,72 @@
         SR[n, hop(s, d)] = value.astype(BF16)
         s_copy(n, hop(s, d), d).start()
 
-    for s in range(4):
-
-        def send_step(n, _):
-            for d in range(2):
-                if s < 3:
-                    send_sum(n, s, d)
-                else:
-
-                    @pl.when(lax.rem(n, 2) == d)
-                    def _():
-                        send_sum(n, s, d)
-
+    def over_chunks(body):
+        def step(n, _):
+            body(n)
             return 0
 
-        lax.fori_loop(0, NB, send_step, 0)
-
-    def finish(n, _):
-        odd = lax.rem(n, 2)
-        value = partial_sum(n, z)
+        lax.fori_loop(0, NB, step, 0)
+
+    def first(n):
+        send_sum(n, 0, 0)
+        send_sum(n, 0, 1)
+
+    def most(s):
+        def body(n):
+            send_sum(n, s, 0)
+
+            @pl.when(lax.rem(n, 2) == 1)
+            def _():
+                send_sum(n, s, 1)
+
+        return body
+
+    def rest(s):
+        def body(n):
+            @pl.when(lax.rem(n, 2) == 0)
+            def _():
+                send_sum(n, s, 1)
+
+        return body
+
+    def fourth(n):
         for d in range(2):
-            last = jnp.where(odd == d, 6, 4 + d)
+
+            @pl.when(lax.rem(n, 2) == d)
+            def _():
+                send_sum(n, 3, d)
+
+    def finish(n):
+        value = partial_sum(n, OWN)
+        for d in range(2):
+            last = jnp.where(lax.rem(n, 2) == d, 6, 4 + d)
             s_copy(n, last, d).wait_recv()
             value = value + RR[n, last].astype(F32)
         out_ref[:, pl.ds(pl.multiple_of(n * FC, FC), FC)] = value.astype(BF16)
+
+    over_chunks(first)
+    lax.fori_loop(6, 8, down, 0)
+    for d in range(2):
+        m_copy(1, d).start()
+    over_chunks(most(1))
+    wait_bytes(RX.at[1, pl.ds(0, NQ - 1)], wrs.at[1])
+    over_chunks(rest(1))
+    over_chunks(most(2))
+    over_chunks(rest(2))
+    over_chunks(fourth)
+
+    wait_bytes(PN.at[0], mrs.at[2])
+    wait_bytes(PN.at[1], mrs.at[3])
+
+    def mix(u, _):
+        c, cols = u // 4, pl.ds(pl.multiple_of(lax.rem(u, 4) * 512, 512), 512)
+        value = PT[y, c, :, cols].astype(F32) + PN[0, c, :, cols].astype(F32) + PN[1, c, :, cols].astype(F32)
+        mix_ref[:, pl.ds(pl.multiple_of(u * 512, 512), 512)] = value.astype(BF16)
         return 0
 
-    lax.fori_loop(0, NB, finish, 0)
-
-    wait_bytes(PM.at[pl.ds(1, NY - 1)], mrs.at[0])
-
-    def mix(u, _):
-        cols = pl.ds(pl.multiple_of(u * 512, 512), 512)
-        value = PT[y, :, cols].astype(F32)
-        for i in range(1, NY):
-            value = value + PM[i, :, cols].astype(F32)
-        mix_ref[:, cols] = value.astype(BF16)
-        return 0
-
     lax.fori_loop(0, D // 512, mix, 0)
+    over_chunks(finish)
 
     for view, sem in (
         (G.at[:, pl.ds(0, 7)], zss),
@@ -508,12 +575,13 @@
         (XO, yss),
         (DN.at[pl.ds(0, NY - 1)], dss),
         (ACT.at[pl.ds(0, NY - 1)], ass),
-        (RX.at[pl.ds(0, NQ - 1)], wss),
+        (RX.at[:, pl.ds(0, NQ - 1)], wss),
         (SR, sss),
-        (PM.at[pl.ds(1, NY - 1)], mss),
+        (PM, mss),
         (KP, hss),
     ):
         wait_bytes(view, sem.at[0])
+    wait_bytes(PN, mss.at[1])
 
 
 def write_out(mix_in, out_in, mix_ref, out_ref):
@@ -563,31 +631,32 @@
             pltpu.VMEM((512, D), BF16),
             pltpu.VMEM((NY, HID, 1024), BF16),
             pltpu.VMEM((NQ, ROWS, NZ * TOK), BF16),
-            pltpu.VMEM((NZ, TOK, NQ * ROWS), BF16),
+            pltpu.VMEM((NZ, TOK, NQ * HALF), BF16),
             pltpu.VMEM((NZ, 8, TOK), F32),
             pltpu.VMEM((NZ, 16, TOK), F32),
             pltpu.VMEM((NQ * ROWS, 2 * HID), F32),
-            pltpu.VMEM((NY, NQ, ROWS, HID), BF16),
-            pltpu.VMEM((NQ, ROWS, 1024), BF16),
-            pltpu.VMEM((NQ, ROWS, 1024), BF16),
+            pltpu.VMEM((NY, 2, NQ, HALF, HID), BF16),
+            pltpu.VMEM((2, NQ, HALF, 1024), BF16),
+            pltpu.VMEM((2, NQ, HALF, 1024), BF16),
             pltpu.VMEM((NB, 7, TOK, FC), BF16),
             pltpu.VMEM((NB, 7, TOK, FC), BF16),
             pltpu.VMEM((2, 128, 128), BF16),
             pltpu.VMEM((2, 2, 384, 128), BF16),
             pltpu.VMEM((2, 2, 384, 128), BF16),
             pltpu.VMEM((256, 512), BF16),
-            pltpu.VMEM((NY, 64, D), BF16),
-            pltpu.VMEM((NY, 64, D), BF16),
+            pltpu.VMEM((NY, 2, 64, D // 2), BF16),
+            pltpu.VMEM((2, 64, D // 2), BF16),
+            pltpu.VMEM((2, 2, 64, D // 2), BF16),
             dma((11,)),
             dma((1,)), dma((C, 7)),
             dma((1,)), dma((7,)),
             dma((1,)), dma((C,)),
             dma((1,)), dma((CE,)),
             dma((1,)), dma((1,)),
-            dma((1,)), dma((4,)),
-            dma((1,)), dma((1,)),
+            dma((1,)), dma((8,)),
+            dma((1,)), dma((2,)),
             dma((1,)), dma((NB, 7)),
-            dma((1,)), dma((1,)),
+            dma((2,)), dma((4,)),
             dma((1,)), dma((1,)),
         ],
         compiler_params=pltpu.CompilerParams(

time: 129 us -> 121 us (0.938); the launches traced: 128 us -> 118 us
  Pallas kernels: 127 us -> 118 us
    pallas_call x1, Pallas kernels: 125 us -> 116 us  [shards(): pl.pallas_call(kernel, out_shape=(jax.ShapeDtypeStruct((64, D), BF16), ja...]
where the time goes in v3:
time: 121 us; the launch traced here: 118 us
  Pallas kernels  118 us (98%)
    pallas_call x1, Pallas kernels, shards(): pl.pallas_call(kernel, out_shape=(jax.ShapeDtypeStruct((64, D), BF16), ja...  116 us

profile of v3, /device:TPU:2, one launch (start us, length us, event | category | flops | bytes accessed | tf_op | source)
XLA Modules:
  0.0 118.4 jit_solution(2628904633216548621)
XLA Ops:
  0.6 115.7 %shard_map.131 = (bf16[64,4096]{1,0:T(8,128)(2,1)}, bf16[128,1024]{1,0:T(8,128)(2,1)}) custom-call(bf16[256,512]{1,0:T(8,128)(2,1)} %q_hbm.1, bf16[256,128]{1,0:T(8,128)(2,1)} %k_hbm.1, bf16[256,128]{1,0:T(8,128)(2,1)} %v_hbm.1, f32[8]{0:T(128)} %sink_ref.1, bf16[512,4096]{1,0:T(8,128)(2,1)} %wo_hbm.1, bf16[128,4096]{1,0:T(8,128)(2,1)} %x_hbm.1, ...), custom_call_target="tpu_custom_call" | custom-call | tf_op jit(solution)/shard_map/pallas_call | solution.py:610
  116.4 2.0 %shard_map.132 = (bf16[64,4096]{1,0:T(8,128)(2,1)}, bf16[128,1024]{1,0:T(8,128)(2,1)}) custom-call(bf16[64,4096]{1,0:T(8,128)(2,1)} %get-tuple-element.4.mix_in, bf16[128,1024]{1,0:T(8,128)(2,1)} %get-tuple-element.5.out_in), custom_call_target="tpu_custom_call" | custom-call | tf_op jit(solution)/shard_map/pallas_call | solution.py:679

commit v4 on v3

--- a/solution.py
+++ b/solution.py
@@ -304,61 +304,65 @@
             def _():
                 x_copy(j, 4 * r + i).start()
 
+    def forward(t, s):
+        j = t - s
+        if s < 3:
+            for d in range(2):
+
+                @pl.when(j == 0)
+                def _():
+                    i_copy(s - 1, d).wait_recv()
+                    i_copy(s, d).start()
+
+                z_copy(j, s - 1, d).wait_recv()
+                z_copy(j, s, d).start()
+            return
+
+        @pl.when(j == 0)
+        def _():
+            i_copy(2, 0).wait_recv()
+            i_copy(2, 1).wait_recv()
+            i_copy(3, 0).start()
+
+        for d in range(2):
+            z_copy(j, 2, d).wait_recv()
+
+            @pl.when(lax.rem(j, 2) == d)
+            def _():
+                z_copy(j, 3, d).start()
+
+    def gather(j):
+        for d in range(2):
+
+            @pl.when(lax.rem(j, 2) == d)
+            def _():
+                z_copy(j, 3, d).wait_recv()
+
+        def step(r, _):
+            pick(j, r)
+            return 0
+
+        lax.fori_loop(0, 2, step, 0)
+        XF[j, q] = XS[j, q]
+
     def tick(t, _):
-        @pl.when(within(t - 3))
-        def _():
-            j = t - 3
-
-            @pl.when(j == 0)
-            def _():
-                i_copy(2, 0).wait_recv()
-                i_copy(2, 1).wait_recv()
-                i_copy(3, 0).start()
-
-            for d in range(2):
-                z_copy(j, 2, d).wait_recv()
-
-                @pl.when(lax.rem(j, 2) == d)
-                def _():
-                    z_copy(j, 3, d).start()
-
-        @pl.when(within(t - 4))
-        def _():
-            j = t - 4
-
-            @pl.when(j == 0)
-            def _():
-                i_copy(3, 0).wait_recv()
-                build_gather()
-
-            for d in range(2):
-
-                @pl.when(lax.rem(j, 2) == d)
-                def _():
-                    z_copy(j, 3, d).wait_recv()
-
-            pick(j, 0)
-
-        for s in (2, 1):
-
-            @pl.when(within(t - s))
-            def _():
-                for d in range(2):
-
-                    @pl.when(t == s)
-                    def _():
-                        i_copy(s - 1, d).wait_recv()
-                        i_copy(s, d).start()
-
-                    z_copy(t - s, s - 1, d).wait_recv()
-                    z_copy(t - s, s, d).start()
-
-            if s == 2:
-
-                @pl.when(within(t - 4))
-                def _():
-                    pick(t - 4, 1)
-                    XF[t - 4, q] = XS[t - 4, q]
+        for s in (3, 2, 1):
+
+            @pl.when((t < 4) & within(t - s))
+            def _():
+                forward(t, s)
+
+        @pl.when(t == 4)
+        def _():
+            i_copy(3, 0).wait_recv()
+            build_gather()
+            gather(0)
+
+        for s in (1, 2, 3):
+
+            @pl.when((t >= 4) & within(t - s))
+            def _():
+                forward(t, s)
 
         @pl.when(t == 1)
         def _():
@@ -369,6 +373,10 @@
         def _():
             for d in range(2):
                 z_copy(t + AHEAD, 0, d).start()
+
+        @pl.when((t > 4) & within(t - 4))
+        def _():
+            gather(t - 4)
 
         @pl.when(within(t - 6))
         def _():
@@ -477,7 +485,7 @@
 
         return 0
 
-    lax.fori_loop(0, 6, down, 0)
+    lax.fori_loop(0, 5, down, 0)
     wait_bytes(RX.at[0, pl.ds(0, NQ - 1)], wrs.at[0])
 
     def partial_sum(n, place):
@@ -546,7 +554,7 @@
         out_ref[:, pl.ds(pl.multiple_of(n * FC, FC), FC)] = value.astype(BF16)
 
     over_chunks(first)
-    lax.fori_loop(6, 8, down, 0)
+    lax.fori_loop(5, 8, down, 0)
     for d in range(2):
         m_copy(1, d).start()
     over_chunks(most(1))
@@ -582,11 +590,6 @@
     ):
         wait_bytes(view, sem.at[0])
     wait_bytes(PN, mss.at[1])
-
-
-def write_out(mix_in, out_in, mix_ref, out_ref):
-    mix_ref[...] = mix_in[...]
-    out_ref[...] = out_in[...]
 
 
 def shards(
@@ -610,8 +613,8 @@
     mixed, combined = pl.pallas_call(
         kernel,
         out_shape=(
-            jax.ShapeDtypeStruct((64, D), BF16),
-            jax.ShapeDtypeStruct((TOK, 1024), BF16),
+            pltpu.VMEM((64, D), BF16),
+            pltpu.VMEM((TOK, 1024), BF16),
         ),
         in_specs=[hbm, hbm, hbm, smem, hbm, hbm, hbm, hbm, hbm, hbm, hbm, hbm],
         out_specs=(vmem, vmem),
@@ -676,15 +679,7 @@
         up_weight.reshape(D // FC, FC, HID),
         down_weight.reshape(HID, D),
     )
-    return pl.pallas_call(
-        write_out,
-        out_shape=(
-            jax.ShapeDtypeStruct((64, D), BF16),
-            jax.ShapeDtypeStruct((TOK, 1024), BF16),
-        ),
-        in_specs=[vmem, vmem],
-        out_specs=(vmem, vmem),
-    )(mixed, combined)
+    return mixed, combined
 
 
 def solution(mesh):

time: 121 us -> 117 us (0.967)
  Pallas kernels: 118 us -> 113 us
  local copies, waits for them, and re-layouts: 0 us -> 1.5 us
    pallas_call x2 -> x1, Pallas kernels: 118 us -> 113 us  [shards(): pl.pallas_call(kernel, out_shape=(pltpu.VMEM((64, D), BF16), pltpu.VMEM((...]
    unnamed x0 -> x2, local copies, waits for them, and re-layouts: none -> 1.5 us
where the time goes in v4:
time: 117 us; the launch traced here: 115 us
  Pallas kernels  113 us (97%)
  local copies, waits for them, and re-layouts  1.5 us (1%)
    pallas_call x1, Pallas kernels, shards(): pl.pallas_call(kernel, out_shape=(pltpu.VMEM((64, D), BF16), pltpu.VMEM((...  113 us

profile of v4, /device:TPU:2, one launch (start us, length us, event | category | flops | bytes accessed | tf_op | source)
XLA Modules:
  0.0 115.0 jit_solution(5424460818767442460)
XLA Ops:
  0.6 112.8 %shard_map.131 = (bf16[64,4096]{1,0:T(8,128)(2,1)S(1)}, bf16[128,1024]{1,0:T(8,128)(2,1)S(1)}) custom-call(bf16[256,512]{1,0:T(8,128)(2,1)} %q_hbm.1, bf16[256,128]{1,0:T(8,128)(2,1)} %k_hbm.1, bf16[256,128]{1,0:T(8,128)(2,1)} %v_hbm.1, f32[8]{0:T(128)} %sink_ref.1, bf16[512,4096]{1,0:T(8,128)(2,1)} %wo_hbm.1, bf16[128,4096]{1,0:T(8,128)(2,1)} %x_hbm.1, ...), custom_call_target="tpu_custom_call" | custom-call | tf_op jit(solution)/shard_map/pallas_call | solution.py:613
  113.5 0.8 copy.16
  114.3 0.7 copy.17

commit v5 on v4

--- a/solution.py
+++ b/solution.py
@@ -19,7 +19,7 @@
 FC = 256
 CE = 7
 C = 9
-AHEAD = 3
+AHEAD = 2
 HID = 256
 NB = 4
 HALF = ROWS // 2
@@ -134,7 +134,7 @@
 
     def a_copy(h, qq, b, i):
         to = wrap(y + i, NY)
-        return remote(ACT.at[y, h, qq], ACT.at[y, h, qq], ass.at[0], ars.at[4 * h + b], at_y(to))
+        return remote(ACT.at[y, h, qq], ACT.at[y, h, qq], ass.at[0], ars.at[8 * h + b], at_y(to))
 
     def w_copy(h, to):
         return remote(YS.at[h, to], RX.at[h, q], wss.at[0], wrs.at[h], at_q(to))
@@ -346,21 +346,21 @@
         XF[j, q] = XS[j, q]
 
     def tick(t, _):
-        for s in (3, 2, 1):
-
-            @pl.when((t < 4) & within(t - s))
-            def _():
-                forward(t, s)
-
         @pl.when(t == 4)
         def _():
             i_copy(3, 0).wait_recv()
             build_gather()
             gather(0)
 
+        for s in (3, 2, 1):
+
+            @pl.when((t <= 4) & within(t - s))
+            def _():
+                forward(t, s)
+
         for s in (1, 2, 3):
 
-            @pl.when((t >= 4) & within(t - s))
+            @pl.when((t > 4) & within(t - s))
             def _():
                 forward(t, s)
 
@@ -377,6 +377,10 @@
         @pl.when((t > 4) & within(t - 4))
         def _():
             gather(t - 4)
+
+        @pl.when(t == C + 4)
+        def _():
+            build_combine()
 
         @pl.when(within(t - 6))
         def _():
@@ -434,29 +438,26 @@
 
     lax.fori_loop(0, C + 6, tick, 0)
 
-    def pair(b):
+    def nth(b):
         chip, core = q // 2, lax.rem(q, 2)
-        apart = (b > 0) & (b < 3)
-        dx = jnp.where(b == 0, 2, jnp.where(b == 3, 0, 1))
-        dc = jnp.where(apart, b - 1, 0)
-        first = lax.rem(chip + dx, 4) * 2 + lax.rem(core + dc, 2)
-        dx = jnp.where(apart, 3, dx)
-        dc = jnp.where(apart, b - 1, 1)
-        return first, lax.rem(chip + dx, 4) * 2 + lax.rem(core + dc, 2)
+        turn, odd = b // 2, lax.rem(b, 2)
+        apart = (turn > 0) & (turn < 3)
+        dx = jnp.where(turn == 0, 2, jnp.where(turn == 3, 0, jnp.where(odd == 0, 1, 3)))
+        dc = jnp.where(apart, turn - 1, odd)
+        return lax.rem(chip + dx, 4) * 2 + lax.rem(core + dc, 2)
 
     def activate(hb, _):
-        h, b = hb // 4, lax.rem(hb, 4)
-        for qq in pair(b):
-            rows = pl.ds(pl.multiple_of(qq * ROWS + h * HALF, 16), HALF)
-            g = jnp.minimum(ACC[rows, 0:HID], CLAMP)
-            u = jnp.clip(ACC[rows, HID : 2 * HID], -CLAMP, CLAMP) + 1.0
-            ACT[y, h, qq] = (u * g * jax.nn.sigmoid(SLOPE * g)).astype(BF16)
-            for i in (2, 1, 3):
-                a_copy(h, qq, b, i).start()
+        h, b = hb // 8, lax.rem(hb, 8)
+        qq = nth(b)
+        rows = pl.ds(pl.multiple_of(qq * ROWS + h * HALF, 16), HALF)
+        g = jnp.minimum(ACC[rows, 0:HID], CLAMP)
+        u = jnp.clip(ACC[rows, HID : 2 * HID], -CLAMP, CLAMP) + 1.0
+        ACT[y, h, qq] = (u * g * jax.nn.sigmoid(SLOPE * g)).astype(BF16)
+        for i in (2, 1, 3):
+            a_copy(h, qq, b, i).start()
         return 0
 
-    lax.fori_loop(0, 8, activate, 0)
-    build_combine()
+    lax.fori_loop(0, 16, activate, 0)
     loads[10].wait()
     wait_bytes(DN.at[pl.ds(0, NY - 1)], drs.at[0])
     for d in range(2):
@@ -465,27 +466,25 @@
         PT[to, d] = (PT[to, d].astype(F32) + PM[d].astype(F32)).astype(BF16)
 
     def down(hb, _):
-        h, b = hb // 4, lax.rem(hb, 4)
-        wait_bytes(ACT.at[pl.ds(0, NY - 1), 0, pl.ds(0, 2)], ars.at[hb])
-        qs = pair(b)
-        block = jnp.zeros((2 * HALF, 1024), F32)
+        h, b = hb // 8, lax.rem(hb, 8)
+        wait_bytes(ACT.at[pl.ds(0, NY - 1), 0, 0], ars.at[hb])
+        qq = nth(b)
+        block = jnp.zeros((HALF, 1024), F32)
         for i in range(NY):
-            acts = jnp.concatenate([ACT[i, h, qq] for qq in qs], axis=0)
-            block = block + jnp.dot(acts, DN[i], preferred_element_type=F32)
-        for i, qq in enumerate(qs):
-            YS[h, qq] = block[i * HALF : (i + 1) * HALF].astype(BF16)
-
-            @pl.when(qq != q)
-            def _():
-                w_copy(h, qq).start()
-
-            @pl.when(qq == q)
-            def _():
-                RX[h, q] = YS[h, q]
+            block = block + jnp.dot(ACT[i, h, qq], DN[i], preferred_element_type=F32)
+        YS[h, qq] = block.astype(BF16)
+
+        @pl.when(qq != q)
+        def _():
+            w_copy(h, qq).start()
+
+        @pl.when(qq == q)
+        def _():
+            RX[h, q] = YS[h, q]
 
         return 0
 
-    lax.fori_loop(0, 5, down, 0)
+    lax.fori_loop(0, 10, down, 0)
     wait_bytes(RX.at[0, pl.ds(0, NQ - 1)], wrs.at[0])
 
     def partial_sum(n, place):
@@ -554,7 +553,7 @@
         out_ref[:, pl.ds(pl.multiple_of(n * FC, FC), FC)] = value.astype(BF16)
 
     over_chunks(first)
-    lax.fori_loop(5, 8, down, 0)
+    lax.fori_loop(10, 16, down, 0)
     for d in range(2):
         m_copy(1, d).start()
     over_chunks(most(1))
@@ -656,7 +655,7 @@
             dma((1,)), dma((C,)),
             dma((1,)), dma((CE,)),
             dma((1,)), dma((1,)),
-            dma((1,)), dma((8,)),
+            dma((1,)), dma((16,)),
             dma((1,)), dma((2,)),
             dma((1,)), dma((NB, 7)),
             dma((2,)), dma((4,)),

time: 117 us -> 115 us (0.983)
  Pallas kernels: 113 us -> 111 us
    pallas_call x1, Pallas kernels: 113 us -> 111 us  [shards(): pl.pallas_call(kernel, out_shape=(pltpu.VMEM((64, D), BF16), pltpu.VMEM((...]
where the time goes in v5:
time: 115 us; the launch traced here: 113 us
  Pallas kernels  111 us (97%)
  local copies, waits for them, and re-layouts  1.5 us (1%)
    pallas_call x1, Pallas kernels, shards(): pl.pallas_call(kernel, out_shape=(pltpu.VMEM((64, D), BF16), pltpu.VMEM((...  111 us

profile of v5, /device:TPU:2, one launch (start us, length us, event | category | flops | bytes accessed | tf_op | source)
XLA Modules:
  0.0 113.3 jit_solution(14501787255784167656)
XLA Ops:
  0.6 111.2 %shard_map.131 = (bf16[64,4096]{1,0:T(8,128)(2,1)S(1)}, bf16[128,1024]{1,0:T(8,128)(2,1)S(1)}) custom-call(bf16[256,512]{1,0:T(8,128)(2,1)} %q_hbm.1, bf16[256,128]{1,0:T(8,128)(2,1)} %k_hbm.1, bf16[256,128]{1,0:T(8,128)(2,1)} %v_hbm.1, f32[8]{0:T(128)} %sink_ref.1, bf16[512,4096]{1,0:T(8,128)(2,1)} %wo_hbm.1, bf16[128,4096]{1,0:T(8,128)(2,1)} %x_hbm.1, ...), custom_call_target="tpu_custom_call" | custom-call | tf_op jit(solution)/shard_map/pallas_call | solution.py:612
  111.8 0.8 copy.16
  112.6 0.7 copy.17
